TPU v7x, 1024 devices: a whole 4x8x16 slice. The times are simulated.
1024 devices in a mesh: dp: 4 (over x), kv: 128 (over z, y), tp: 2 (over core).
Axes of the slice: x: 4, y: 8, z: 16, core: 2. Of those that a mesh axis runs over, the one named last changes fastest.
Arguments:
- tokens: bfloat16 [32, 2048], P('dp', 'kv'), may hold values from -6 to 6
- lengths: int32 [32], P('dp'), may hold values from 1 to 32767, as said below
- query_weight: bfloat16 [2048, 2048], P('kv', 'tp'), may hold values from -0.125 to 0.125
- key_weight: bfloat16 [2048, 256], P('kv', 'tp'), may hold values from -0.125 to 0.125
- value_weight: bfloat16 [2048, 256], P('kv', 'tp'), may hold values from -0.125 to 0.125
- query_gain: float32 [64], replicated, may hold values from 0.1 to 1.9
- key_gain: float32 [64], replicated, may hold values from 0.1 to 1.9
- lambdas: float32 [16], P('tp'), may hold values from 0.3 to 0.8
- head_gain: float32 [128], replicated, may hold values from 0.1 to 1.9
- out_weight: bfloat16 [2048, 2048], P('tp', 'kv'), may hold values from -0.125 to 0.125
- cache_keys: bfloat16 [32, 32768, 2, 128], P('dp', 'kv', 'tp'), may hold values from -400 to 400
- cache_values: bfloat16 [32, 32768, 2, 128], P('dp', 'kv', 'tp'), may hold values from -6 to 6
Outputs:
- mixed: bfloat16 [32, 2048], P('dp', 'kv')
- new_keys: bfloat16 [32, 2, 128], P('dp', 'tp')
- new_values: bfloat16 [32, 2, 128], P('dp', 'tp')
Inputs may be any that keep to these rules, and one draw needn't show every extreme that they name: `lengths`: of each index of dp's 8 sequences, the first has 32512 or more cached positions, the second fewer than 16, the others half of 32768 or more.
All inputs are finite; a program needn't handle non-finite values.
Results may differ from a plain program's by a relative error of at most 0.023.
Values may be sent and summed in bfloat16 or wider, within the bound.
A program may use at most 64 MiB of HBM per device.

v0:
```python
import functools
import math

import jax
import jax.numpy as jnp
from jax import lax
from jax.sharding import Mesh
from jax.sharding import PartitionSpec as P

KV = ("kv_0", "kv_1")


epsilon = 1e-06
rotary_base = 10000.0
masked_score = -1e30
output_scale = 0.2 + 0.6 * math.exp(-0.3)


def one_axis_at_a_time(x, axes):
    return functools.reduce(lax.psum, axes, x)


def gathered_once(x, axis):
    leaves = jax.tree.leaves(x)
    sequence = sorted(range(len(leaves)), key=lambda k: -leaves[k].size)
    width = (1, *leaves[sequence[0]].shape)[-1]
    lines = [
        jnp.pad(leaves[k].reshape(-1), (0, -leaves[k].size % width)).reshape(-1, width)
        for k in sequence
    ]
    both, at, found = (lax.all_gather(jnp.concatenate(lines), axis), 0, {})
    for k, line in zip(sequence, lines):
        slab = both[:, at : at + len(line)].reshape(len(both), -1)
        found[k] = slab[:, : leaves[k].size].reshape(-1, *leaves[k].shape)
        at += len(line)
    numbers = iter(range(len(leaves)))
    return jax.tree.map(lambda _: found[next(numbers)], x)


def joined_all(x, axes, combine):
    for axis in axes:
        pieces = gathered_once(x, axis)
        x = jax.tree.map(lambda part: part[0], pieces)
        for k in range(1, lax.axis_size(axis)):
            x = combine(x, jax.tree.map(lambda part: part[k], pieces))
    return x


def total_of_pieces(x, axis):
    return lax.all_gather(x, axis).astype(jnp.float32).sum(0)


def new_entries(proj_query, proj_key, proj_value, query_gain, key_gain, lengths):
    rows = proj_query.shape[0]
    head_dim = query_gain.shape[0]
    half_dim = head_dim // 2
    frequency = rotary_base ** (-jnp.arange(half_dim, dtype=jnp.float32) / half_dim)
    angle = lengths.astype(jnp.float32)[:, None, None, None] * frequency
    cosine_term = jnp.cos(angle)
    sine_term = jnp.sin(angle)

    def turned(pieces, gain):
        normed = (
            pieces * lax.rsqrt(jnp.mean(pieces * pieces, axis=-1, keepdims=True) + epsilon) * gain
        )
        lower_part = normed[..., :half_dim]
        upper_part = normed[..., half_dim:]
        return jnp.concatenate(
            [
                lower_part * cosine_term - upper_part * sine_term,
                upper_part * cosine_term + lower_part * sine_term,
            ],
            axis=-1,
        )

    queries = turned(proj_query.reshape(rows, -1, 2, head_dim), query_gain).astype(jnp.bfloat16)
    new_keys = turned(proj_key.reshape(rows, -1, 2, head_dim), key_gain).astype(jnp.bfloat16)
    new_values = proj_value.reshape(rows, -1, 2 * head_dim).astype(jnp.bfloat16)
    return (queries, new_keys.reshape(rows, -1, 2 * head_dim), new_values)


def combine_parts(earlier, latter):
    highest_first, totals_first, weighted_first = earlier
    highest_second, totals_second, weighted_second = latter
    highest = jnp.maximum(highest_first, highest_second)
    factor_first = jnp.exp(highest_first - highest)
    factor_second = jnp.exp(highest_second - highest)
    totals = totals_first * factor_first + totals_second * factor_second
    weighted = weighted_first * factor_first[..., None] + weighted_second * factor_second[..., None]
    return (highest, totals, weighted)


def body(
    tokens,
    lengths,
    query_weight,
    key_weight,
    value_weight,
    query_gain,
    key_gain,
    lambdas,
    head_gain,
    out_weight,
    cache_keys,
    cache_values,
):
    partial_query = jnp.dot(tokens, query_weight, preferred_element_type=jnp.float32)
    partial_key = jnp.dot(tokens, key_weight, preferred_element_type=jnp.float32)
    partial_value = jnp.dot(tokens, value_weight, preferred_element_type=jnp.float32)
    proj_query, proj_key, proj_value = (
        one_axis_at_a_time(partial_query, KV),
        one_axis_at_a_time(partial_key, KV),
        one_axis_at_a_time(partial_value, KV),
    )
    queries, new_keys, new_values = new_entries(
        proj_query, proj_key, proj_value, query_gain, key_gain, lengths
    )
    rows, positions, kv_heads, width = cache_keys.shape
    head_dim = width // 2
    scale = head_dim ** (-0.5)
    queries = queries.reshape(rows, kv_heads, -1, 2, head_dim)
    keys_split = cache_keys.reshape(rows, positions, kv_heads, 2, head_dim)
    scores = (
        jnp.einsum("skgtd,spktd->skgtp", queries, keys_split, preferred_element_type=jnp.float32)
        * scale
    )
    offset = lax.axis_index(KV) * positions
    position_ids = offset + jnp.arange(positions, dtype=jnp.int32)
    valid = (position_ids[None, :] < lengths[:, None])[:, None, None, None, :]
    local_highest = jnp.max(jnp.where(valid, scores, masked_score), axis=-1)
    expo = jnp.where(valid, jnp.exp(scores - local_highest[..., None]), 0.0)
    totals = jnp.sum(expo, axis=-1)
    weighted = jnp.einsum(
        "skgtp,spke->skgte",
        expo.astype(jnp.bfloat16),
        cache_values,
        preferred_element_type=jnp.float32,
    )
    local_totals = totals
    local_weighted = weighted
    highest, totals, weighted = joined_all(
        (local_highest, local_totals, local_weighted), KV, combine_parts
    )
    own_score = (
        jnp.einsum(
            "skgtd,sktd->skgt",
            queries,
            new_keys.reshape(rows, kv_heads, 2, head_dim),
            preferred_element_type=jnp.float32,
        )
        * scale
    )
    final_highest = jnp.maximum(highest, own_score)
    rescale = jnp.exp(highest - final_highest)
    own_weight = jnp.exp(own_score - final_highest)
    totals = totals * rescale + own_weight
    weighted = weighted * rescale[..., None]
    weighted = (
        weighted + own_weight[..., None] * new_values.astype(jnp.float32)[:, :, None, None, :]
    )
    heads = weighted / totals[..., None]
    gaps = heads[..., 0, :] - lambdas.reshape(kv_heads, -1)[None, :, :, None] * heads[..., 1, :]
    normed = gaps * lax.rsqrt(jnp.mean(gaps * gaps, axis=-1, keepdims=True) + epsilon) * head_gain
    attended = (normed * output_scale).astype(jnp.bfloat16).reshape(rows, -1)
    partial_out = jnp.dot(attended, out_weight, preferred_element_type=jnp.float32)
    mixed = (
        total_of_pieces(partial_out.astype(jnp.bfloat16), "tp")
        .astype(jnp.float32)
        .astype(jnp.bfloat16)
    )
    return (mixed, new_keys, new_values)


def solution(mesh):
    finer = Mesh(
        mesh.devices.reshape(mesh.shape["dp"], 16, 8, mesh.shape["tp"]),
        ("dp", "kv_0", "kv_1", "tp"),
    )
    in_specs = (
        P("dp", KV),
        P("dp"),
        P(KV, "tp"),
        P(KV, "tp"),
        P(KV, "tp"),
        P(),
        P(),
        P("tp"),
        P(),
        P("tp", KV),
        P("dp", KV, "tp", None),
        P("dp", KV, "tp", None),
    )
    out_specs = (P("dp", KV), P("dp", "tp", None), P("dp", "tp", None))
    return jax.shard_map(body, mesh=finer, in_specs=in_specs, out_specs=out_specs, check_vma=False)
```

profile of v0, /device:TPU:1, one launch (start us, length us, event | category | flops | bytes accessed | tf_op | source)
XLA Modules:
  0.0 232.9 jit_solution(118880303075792318)
XLA Ops:
  7.3 0.7 convert_element_type.45
  7.9 0.7 broadcast_compare_fusion
  8.7 0.8 fusion.176
  9.5 0.8 fusion.177
  10.3 0.9 fusion.175
  11.2 55.9 %all-reduce = (f32[8,1024]{1,0:T(8,128)S(1)}, f32[8,128]{1,0:T(8,128)S(1)}, f32[8,128]{1,0:T(8,128)S(1)}) all-reduce(f32[8,1024]{1,0:T(8,128)S(1)} %fusion.175, f32[8,128]{1,0:T(8,128)S(1)} %fusion.176, f32[8,128]{1,0:T(8,128)S(1)} %fusion.177), channel_id=1, replica_groups=mesh['dp'=4,'kv_0'=16,'kv_1'=8,'tp'=2] {'kv_0'}, use_global_device_ids=true, to_apply=%region_0.0 | all-reduce | flops 10240 | bytes 81920 | tf_op jit(solution)/shard_map/psum | solution.py:20
  67.2 24.1 %all-reduce.1 = (f32[8,8,2,64]{3,1,2,0:T(8,128)S(1)}, f32[8,1,2,64]{3,2,0,1:T(2,128)S(1)}, bf16[8,128]{1,0:T(8,128)(2,1)S(1)}) all-reduce(f32[8,8,2,64]{3,1,2,0:T(8,128)S(1)} %copy.70, f32[8,1,2,64]{3,2,0,1:T(2,128)S(1)} %reshape.3950, f32[8,128]{1,0:T(8,128)S(1)} %get-tuple-element.21), channel_id=1, replica_groups=mesh['dp'=4,'kv_0'=16,'kv_1'=8,'tp'=2] {'kv_1'}, use_global_device_ids=true, to_apply=%region_1.0 | all-reduce | flops 10240 | bytes 79872 | tf_op jit(solution)/shard_map/psum | solution.py:20
  91.5 1.2 copy.71
  94.4 0.6 maximum_bitcast_fusion
  95.4 0.7 convert_element_type.51
  96.4 74.5 %all-gather.7.cloned.1.call-done = f32[16,130,128]{2,1,0:T(8,128)} async-done(((f32[1,130,128]{2,1,0:T(8,128)}), f32[16,130,128]{2,1,0:T(8,128)}) %all-gather.7.cloned.1.call-update) | async-done | bytes 1064976 | tf_op jit(solution)/shard_map/all_gather | solution.py:31
  170.9 0.7 fusion.169
  171.6 0.9 fusion.95
  172.5 0.7 fusion.168
  173.3 0.7 fusion.166
  174.0 0.7 fusion.164
  174.7 0.7 fusion.162
  175.4 0.7 fusion.160
  176.1 0.7 fusion.158
  176.8 0.7 fusion.156
  177.5 1.9 fusion.8
  179.4 20.4 %all-gather.4 = f32[8,130,128]{2,1,0:T(8,128)S(1)} all-gather(f32[1,130,128]{2,1,0:T(8,128)S(1)} %maximum_bitcast_fusion.1), channel_id=3, replica_groups=mesh['dp'=4,'kv_0'=16,'kv_1'=8,'tp'=2] {'kv_1'}, dimensions={0}, use_global_device_ids=true | all-gather | bytes 599040 | tf_op jit(solution)/shard_map/all_gather | solution.py:31
  207.1 18.4 %all-gather.2 = bf16[16,16]{1,0:T(8,128)(2,1)S(1)} all-gather(bf16[8,16]{1,0:T(8,128)(2,1)S(1)} %convolution_convert_fusion), channel_id=4, replica_groups=mesh['dp'=4,'kv_0'=16,'kv_1'=8,'tp'=2] {'tp'}, dimensions={0}, use_global_device_ids=true | all-gather | bytes 768 | tf_op jit(solution)/shard_map/all_gather | solution.py:50
  225.5 0.6 bitcast_reduce_fusion
  (107 shorter events, 9.8 us)
Async XLA Ops:
  7.2 86.5 %copy-start = (bf16[8,256,1,128]{3,1,2,0:T(8,128)(2,1)S(1)}, bf16[8,256,1,128]{3,1,2,0:T(8,128)(2,1)}, u32[]{:S(2)}) copy-start(bf16[8,256,1,128]{3,1,2,0:T(8,128)(2,1)} %param.23) | copy-start | bytes 1572868
  7.2 85.6 %copy-start.4 = (f32[64]{0:T(128)S(1)}, f32[64]{0:T(128)}, u32[]{:S(2)}) copy-start(f32[64]{0:T(128)} %param.17) | copy-start | bytes 772
  7.2 163.7 %all-gather.7.cloned.1.call-start = ((), (), s32[]{:S(2)}) async-start(), calls=%async_computation | async-start | bytes 1183744 | tf_op jit(solution)/shard_map/all_gather | solution.py:31
  91.3 4.8 %copy-start.3 = (bf16[8,128]{1,0:T(8,128)(2,1)}, bf16[8,128]{1,0:T(8,128)(2,1)S(1)}, u32[]{:S(2)}) copy-start(bf16[8,128]{1,0:T(8,128)(2,1)S(1)} %get-tuple-element.24) | copy-start | bytes 6148
  93.0 2.1 copy-start.6
  93.0 3.1 %copy-start.2 = (f32[8]{0:T(128)S(1)}, f32[8]{0:T(128)}, u32[]{:S(2)}) copy-start(f32[8]{0:T(128)} %param.19) | copy-start | bytes 100
  93.0 3.1 %copy-start.5 = (f32[128]{0:T(128)S(1)}, f32[128]{0:T(128)}, u32[]{:S(2)}) copy-start(f32[128]{0:T(128)} %param.20) | copy-start | bytes 1540
  203.7 3.2 %copy-start.1 = (bf16[1024,16]{0,1:T(8,128)(2,1)S(1)}, bf16[1024,16]{0,1:T(8,128)(2,1)}, u32[]{:S(2)}) copy-start(bf16[1024,16]{0,1:T(8,128)(2,1)} %param.21) | copy-start | bytes 98308
Sparse Core Ops, SparseCore 0:
  95.2 75.6 all-gather.6
where the time goes:
time: 234 us; the launch traced here: 233 us
  blocking collectives  119 us (51%)
  waiting for transfers between devices  74.5 us (32%)
  between operations  14.5 us (6%)
  other arithmetic  12.7 us (5%)
  local copies, waits for them, and re-layouts  9.02 us (4%)
  matrix products  3.48 us (1%)
    psum x2, blocking collectives, one_axis_at_a_time(): return functools.reduce(lax.psum, axes, x)  79.9 us
    all_gather x1, waiting for transfers between devices, gathered_once(): both, at, found = (lax.all_gather(jnp.concatenate(lines), axis), 0, {})  74.5 us
    all_gather x1, blocking collectives, gathered_once(): both, at, found = (lax.all_gather(jnp.concatenate(lines), axis), 0, {})  20.4 us
    all_gather x1, blocking collectives, total_of_pieces(): return lax.all_gather(x, axis).astype(jnp.float32).sum(0)  18.4 us
    squeeze x42, local copies, waits for them, and re-layouts, joined_all(): x = combine(x, jax.tree.map(lambda part: part[k], pieces))  5.33 us
    exp x7, other arithmetic, combine_parts(): factor_second = jnp.exp(highest_second - highest)  4.93 us
  transfers between devices with their start and end apart: 1, of which 1 were waited for; matrix products, arithmetic and copies ran while one was open for 1% of the time, Pallas kernels for 0%

commit v1 on v0

v1 whole, which is shorter than its diff:
```python
import functools
import math

import jax
import jax.numpy as jnp
import numpy as np
from jax import lax
from jax.experimental import pallas as pl
from jax.experimental.pallas import tpu as pltpu
from jax.sharding import Mesh
from jax.sharding import PartitionSpec as P

KV = ("kv_0", "kv_1")
MESH = pl.DeviceIdType.MESH

epsilon = 1e-06
rotary_base = 10000.0
masked_score = -1e30
output_scale = 0.2 + 0.6 * math.exp(-0.3)
F32 = jnp.float32
BF16 = jnp.bfloat16


def far_first(n):
    return sorted(range(1, n), key=lambda k: -min(k, n - k))


def near_first(n):
    return sorted(range(1, n), key=lambda k: min(k, n - k))


def kernel(
    nz,
    ny,
    tok_hbm,
    len_hbm,
    wq_hbm,
    wk_hbm,
    wv_hbm,
    qg_hbm,
    kg_hbm,
    lam_hbm,
    hg_hbm,
    ow_hbm,
    ck_hbm,
    cv_hbm,
    freq_hbm,
    mixed_ref,
    nk_ref,
    nv_ref,
    tok,
    wts,
    lens,
    gains,
    lams,
    hgain,
    freq,
    outw,
    ck,
    cv,
    pbuf,
    yrecv,
    zbuf,
    qbuf,
    kvbuf,
    bmsg,
    brecv,
    zw,
    zst,
    attbuf,
    tsend,
    trecv,
    load_sem,
    send_sem,
    recv_sem,
    q_sem,
):
    y = lax.axis_index("kv_1")
    z = lax.axis_index("kv_0")
    core = lax.axis_index("tp")
    positions = ck.shape[1]

    def y_at(k):
        return lax.rem(y + k, ny)

    def z_at(k):
        return lax.rem(z + k, nz)

    barrier = pltpu.get_barrier_semaphore()
    for k in far_first(nz):
        pl.semaphore_signal(barrier, 1, device_id={"kv_0": z_at(k)}, device_id_type=MESH)
    for k in far_first(ny):
        pl.semaphore_signal(barrier, 1, device_id={"kv_1": y_at(k)}, device_id_type=MESH)
    pl.semaphore_signal(barrier, 1, device_id={"tp": 1 - core}, device_id_type=MESH)

    width_q = wq_hbm.shape[1]
    loads = [
        pltpu.make_async_copy(tok_hbm, tok, load_sem.at[0]),
        pltpu.make_async_copy(wq_hbm, wts.at[:, pl.ds(0, width_q)], load_sem.at[1]),
        pltpu.make_async_copy(wk_hbm, wts.at[:, pl.ds(width_q, 128)], load_sem.at[2]),
        pltpu.make_async_copy(wv_hbm, wts.at[:, pl.ds(width_q + 128, 128)], load_sem.at[3]),
        pltpu.make_async_copy(len_hbm, lens, load_sem.at[4]),
        pltpu.make_async_copy(qg_hbm, gains.at[0], load_sem.at[5]),
        pltpu.make_async_copy(kg_hbm, gains.at[1], load_sem.at[6]),
        pltpu.make_async_copy(lam_hbm, lams, load_sem.at[7]),
        pltpu.make_async_copy(hg_hbm, hgain, load_sem.at[8]),
        pltpu.make_async_copy(freq_hbm, freq, load_sem.at[9]),
        pltpu.make_async_copy(ck_hbm, ck, load_sem.at[10]),
        pltpu.make_async_copy(cv_hbm, cv, load_sem.at[11]),
    ]
    heads = width_q // 128
    columns = ow_hbm.shape[0]
    for h in range(heads):
        loads.append(
            pltpu.make_async_copy(
                ow_hbm.at[:, pl.ds(128 * h, 128)],
                outw.at[pl.ds(columns * h, columns)],
                load_sem.at[12 + h],
            )
        )
    for load in loads:
        load.start()

    def send(src, dst, which, axis, target, recv=None):
        copy = pltpu.make_async_remote_copy(
            src_ref=src,
            dst_ref=dst,
            send_sem=send_sem.at[which],
            recv_sem=recv_sem.at[which] if recv is None else recv,
            device_id={axis: target},
            device_id_type=MESH,
        )
        copy.start()

    def all_of(ref, which):
        return pltpu.make_async_remote_copy(
            src_ref=ref,
            dst_ref=ref,
            send_sem=send_sem.at[which],
            recv_sem=recv_sem.at[which],
            device_id={"tp": 1 - core},
            device_id_type=MESH,
        )

    for load in loads[:4]:
        load.wait()
    partial = jnp.dot(tok[...], wts[...], preferred_element_type=F32)
    blocks = heads + 2
    for c in range(blocks):
        pbuf[:, c, :] = partial[:, 128 * c : 128 * (c + 1)]

    pl.semaphore_wait(barrier, (ny - 1) + (nz - 1) + 1)

    for k in far_first(ny):
        send(pbuf.at[y_at(k)], yrecv.at[k - 1], 0, "kv_1", y_at(k))

    for load in loads[4:10]:
        load.wait()
    lane = lax.broadcasted_iota(jnp.int32, (blocks, 128), 1)
    row = lax.broadcasted_iota(jnp.int32, (blocks, 128), 0)
    gain_q = jnp.concatenate([gains[0], gains[0]], axis=1)
    gain_k = jnp.concatenate([gains[1], gains[1]], axis=1)
    gain = jnp.where(row < heads, gain_q, gain_k)
    angle = lens[y].astype(F32) * freq[...]
    cosine = jnp.cos(angle)
    sine = jnp.sin(angle)
    head_row = lax.broadcasted_iota(jnp.int32, (heads, 128), 0)
    lam = jnp.zeros((heads, 128), F32)
    for h in range(heads):
        lam = jnp.where(head_row == h, lams[h], lam)

    all_of(yrecv, 0).wait_recv()
    total = pbuf[y]
    for k in range(ny - 1):
        total = total + yrecv[k]

    zbuf[z] = total
    for k in far_first(nz):
        send(zbuf.at[z], zbuf.at[z], 1, "kv_0", z_at(k))
    all_of(zbuf.at[pl.ds(0, nz - 1)], 1).wait_recv()
    proj = zbuf[0]
    for k in range(1, nz):
        proj = proj + zbuf[k]

    low = lane < 64
    squares = proj * proj
    mean_low = jnp.sum(jnp.where(low, squares, 0.0), axis=1, keepdims=True) / 64
    mean_high = jnp.sum(jnp.where(low, 0.0, squares), axis=1, keepdims=True) / 64
    inverse = jnp.where(low, lax.rsqrt(mean_low + epsilon), lax.rsqrt(mean_high + epsilon))
    normed = proj * inverse * gain
    partner = jnp.where(
        lax.rem(lane, 64) < 32, -pltpu.roll(normed, 96, 1), pltpu.roll(normed, 32, 1)
    )
    rotated = normed * cosine + partner * sine
    qbuf[y] = rotated[:heads].astype(BF16)
    kvbuf[y] = jnp.concatenate([rotated[heads : heads + 1], proj[heads + 1 :]], axis=0)
    for k in far_first(ny):
        send(qbuf.at[y], qbuf.at[y], 2, "kv_1", y_at(k), q_sem.at[k - 1])
    for k in far_first(ny):
        send(kvbuf.at[y], kvbuf.at[y], 3, "kv_1", y_at(k))

    scale = 64 ** (-0.5)
    rows2 = 2 * heads
    wide_lane = lax.broadcasted_iota(jnp.int32, (rows2, 128), 1)
    wide_row = lax.broadcasted_iota(jnp.int32, (rows2, 128), 0)
    eye = wide_lane == wide_row
    half_low = lax.broadcasted_iota(jnp.int32, (heads, 128), 1) < 64
    position_ids = (z * ny + y) * positions + lax.broadcasted_iota(
        jnp.int32, (rows2, positions), 1
    )

    def to_row(column):
        return jnp.sum(jnp.where(eye, column, 0.0), axis=0, keepdims=True)

    def to_column(values):
        return jnp.sum(jnp.where(eye, values, 0.0), axis=1, keepdims=True)

    def two_maps(query):
        return jnp.concatenate(
            [jnp.where(half_low, query, 0.0), jnp.where(half_low, 0.0, query)], axis=0
        )

    def attend(s):
        query = two_maps(qbuf[s].astype(F32)).astype(BF16)
        scores = (
            lax.dot_general(query, ck[s], (((1,), (1,)), ((), ())), preferred_element_type=F32)
            * scale
        )
        valid = position_ids < lens[s]
        highest = jnp.max(jnp.where(valid, scores, masked_score), axis=1, keepdims=True)
        expo = jnp.where(valid, jnp.exp(scores - highest), 0.0)
        count = jnp.sum(expo, axis=1, keepdims=True)
        bmsg[s, pl.ds(0, rows2), :] = jnp.dot(
            expo.astype(BF16), cv[s], preferred_element_type=F32
        )
        bmsg[s, pl.ds(rows2, 2), :] = jnp.concatenate([to_row(highest), to_row(count)], axis=0)

    for load in loads[10:12]:
        load.wait()
    attend(y)
    for k in near_first(ny):
        s = lax.rem(y + ny - k, ny)
        pltpu.make_async_remote_copy(
            src_ref=qbuf.at[s],
            dst_ref=qbuf.at[s],
            send_sem=send_sem.at[2],
            recv_sem=q_sem.at[k - 1],
            device_id={"kv_1": s},
            device_id_type=MESH,
        ).wait_recv()
        attend(s)
        send(bmsg.at[s], brecv.at[k - 1], 4, "kv_1", s)

    own_query = two_maps(qbuf[y].astype(F32))
    own_key = kvbuf[y, pl.ds(0, 1), :].astype(BF16).astype(F32)
    own_value = kvbuf[y, pl.ds(1, 1), :].astype(BF16).astype(F32)
    own_score = to_row(jnp.sum(own_query * own_key, axis=1, keepdims=True) * scale)

    all_of(brecv, 4).wait_recv()
    parts = [bmsg[y]] + [brecv[k] for k in range(ny - 1)]
    highs = [part[rows2 : rows2 + 1] for part in parts]
    high = functools.reduce(jnp.maximum, highs)
    count = jnp.zeros_like(high)
    weighted = jnp.zeros((rows2, 128), F32)
    for part, one in zip(parts, highs):
        factor = jnp.exp(one - high)
        count = count + factor * part[rows2 + 1 :]
        weighted = weighted + to_column(factor) * part[:rows2]
    zw[z] = weighted.astype(BF16)
    zst[z] = jnp.concatenate([high, count], axis=0)
    for k in far_first(nz):
        send(zst.at[z], zst.at[z], 6, "kv_0", z_at(k))
        send(zw.at[z], zw.at[z], 5, "kv_0", z_at(k))
    all_of(zst.at[pl.ds(0, nz - 1)], 6).wait_recv()
    stats = [zst[k] for k in range(nz)]
    high = own_score
    for stat in stats:
        high = jnp.maximum(high, stat[:1])
    own_weight = jnp.exp(own_score - high)
    count = own_weight
    factors = []
    for stat in stats:
        factor = jnp.exp(stat[:1] - high)
        factors.append(factor)
        count = count + factor * stat[1:]
    share = 1.0 / count
    attention = to_column(own_weight * share) * own_value
    columns_of = [to_column(factor * share) for factor in factors]
    all_of(zw.at[pl.ds(0, nz - 1)], 5).wait_recv()
    for k in range(nz):
        attention = attention + columns_of[k] * zw[k].astype(F32)
    gaps = attention[:heads] - lam * attention[heads:]
    mean = jnp.sum(gaps * gaps, axis=1, keepdims=True) / 128
    attended = gaps * lax.rsqrt(mean + epsilon) * hgain[...] * output_scale
    attbuf[y] = attended.astype(BF16)
    for k in far_first(ny):
        send(attbuf.at[y], attbuf.at[y], 7, "kv_1", y_at(k))

    all_of(kvbuf.at[pl.ds(0, ny - 1)], 3).wait_recv()
    for s in range(ny):
        nk_ref[pl.ds(s, 1), :] = kvbuf[s, pl.ds(0, 1), :].astype(BF16)
        nv_ref[pl.ds(s, 1), :] = kvbuf[s, pl.ds(1, 1), :].astype(BF16)
    for load in loads[12:]:
        load.wait()

    all_of(attbuf.at[pl.ds(0, ny - 1)], 7).wait_recv()
    rows = jnp.concatenate([attbuf[s].astype(F32) for s in range(ny)], axis=0).astype(BF16)
    product = lax.dot_general(
        rows, outw[...], (((1,), (1,)), ((), ())), preferred_element_type=F32
    )
    out_row = lax.broadcasted_iota(jnp.int32, product.shape, 0)
    out_lane = lax.broadcasted_iota(jnp.int32, product.shape, 1)
    product = jnp.where(lax.rem(out_row, heads) == out_lane // columns, product, 0.0)
    summed = jnp.sum(product.reshape(ny, heads, 128), axis=1)
    step = columns
    while step < 128:
        summed = summed + pltpu.roll(summed, step, 1)
        step *= 2
    tsend[...] = summed.astype(BF16)
    send(tsend, trecv, 8, "tp", 1 - core)
    all_of(trecv, 8).wait_recv()
    mixed = tsend[...].astype(F32) + trecv[...].astype(F32)
    mixed_ref[...] = mixed[:, :columns].astype(BF16)

    for which, ref in (
        (0, yrecv),
        (1, zbuf.at[pl.ds(0, nz - 1)]),
        (2, qbuf.at[pl.ds(0, ny - 1)]),
        (3, kvbuf.at[pl.ds(0, ny - 1)]),
        (4, brecv),
        (5, zw.at[pl.ds(0, nz - 1)]),
        (6, zst.at[pl.ds(0, nz - 1)]),
        (7, attbuf.at[pl.ds(0, ny - 1)]),
        (8, trecv),
    ):
        all_of(ref, which).wait_send()


def body(
    nz,
    ny,
    tokens,
    lengths,
    query_weight,
    key_weight,
    value_weight,
    query_gain,
    key_gain,
    lambdas,
    head_gain,
    out_weight,
    cache_keys,
    cache_values,
):
    sequences, positions = cache_keys.shape[:2]
    depth, width_q = query_weight.shape
    heads = width_q // 128
    rows2 = 2 * heads
    columns = out_weight.shape[1]
    half = query_gain.shape[0] // 2
    frequency = rotary_base ** (-np.arange(half, dtype=np.float64) / half)
    freq = jnp.asarray(np.tile(frequency, 4).astype(np.float32)[None, :])
    blocks = heads + 2
    any_space = pl.BlockSpec(memory_space=pl.ANY)
    vmem = pl.BlockSpec(memory_space=pltpu.VMEM)
    mixed, new_keys, new_values = pl.pallas_call(
        functools.partial(kernel, nz, ny),
        name="decode_step",
        out_shape=(
            jax.ShapeDtypeStruct((sequences, columns), BF16),
            jax.ShapeDtypeStruct((sequences, 128), BF16),
            jax.ShapeDtypeStruct((sequences, 128), BF16),
        ),
        in_specs=[any_space] * 13,
        out_specs=(vmem, vmem, vmem),
        scratch_shapes=[
            pltpu.VMEM((sequences, depth), BF16),
            pltpu.VMEM((depth, width_q + 256), BF16),
            pltpu.SMEM((sequences,), jnp.int32),
            pltpu.VMEM((2, 1, 64), F32),
            pltpu.SMEM((heads,), F32),
            pltpu.VMEM((1, 128), F32),
            pltpu.VMEM((1, 128), F32),
            pltpu.VMEM((heads * columns, 128), BF16),
            pltpu.VMEM((sequences, positions, 128), BF16),
            pltpu.VMEM((sequences, positions, 128), BF16),
            pltpu.VMEM((sequences, blocks, 128), F32),
            pltpu.VMEM((ny - 1, blocks, 128), F32),
            pltpu.VMEM((nz, blocks, 128), F32),
            pltpu.VMEM((ny, heads, 128), BF16),
            pltpu.VMEM((ny, 2, 128), F32),
            pltpu.VMEM((ny, rows2 + 2, 128), F32),
            pltpu.VMEM((ny - 1, rows2 + 2, 128), F32),
            pltpu.VMEM((nz, rows2, 128), BF16),
            pltpu.VMEM((nz, 2, 128), F32),
            pltpu.VMEM((ny, heads, 128), BF16),
            pltpu.VMEM((sequences, 128), BF16),
            pltpu.VMEM((sequences, 128), BF16),
            pltpu.SemaphoreType.DMA((12 + heads,)),
            pltpu.SemaphoreType.DMA((9,)),
            pltpu.SemaphoreType.DMA((9,)),
            pltpu.SemaphoreType.DMA((ny - 1,)),
        ],
        compiler_params=pltpu.CompilerParams(collective_id=0, has_side_effects=True),
    )(
        tokens,
        lengths,
        query_weight,
        key_weight,
        value_weight,
        query_gain.reshape(1, -1),
        key_gain.reshape(1, -1),
        lambdas,
        head_gain.reshape(1, -1),
        out_weight.T,
        cache_keys.reshape(sequences, positions, 128),
        cache_values.reshape(sequences, positions, 128),
        freq,
    )
    return (
        mixed,
        new_keys.reshape(sequences, 1, 128),
        new_values.reshape(sequences, 1, 128),
    )


def solution(mesh):
    ny = 8
    nz = mesh.shape["kv"] // ny
    finer = Mesh(
        mesh.devices.reshape(mesh.shape["dp"], nz, ny, mesh.shape["tp"]),
        ("dp", "kv_0", "kv_1", "tp"),
    )
    in_specs = (
        P("dp", KV),
        P("dp"),
        P(KV, "tp"),
        P(KV, "tp"),
        P(KV, "tp"),
        P(),
        P(),
        P("tp"),
        P(),
        P("tp", KV),
        P("dp", KV, "tp", None),
        P("dp", KV, "tp", None),
    )
    out_specs = (P("dp", KV), P("dp", "tp", None), P("dp", "tp", None))
    return jax.shard_map(
        functools.partial(body, nz, ny),
        mesh=finer,
        in_specs=in_specs,
        out_specs=out_specs,
        check_vma=False,
    )
```

time: 234 us -> 62.1 us (0.27)
  blocking collectives: 119 us -> 0 us
  waiting for transfers between devices: 74.5 us -> 0 us
  Pallas kernels: 0 us -> 58.6 us
  between operations: 14.5 us -> 0.65 us
  other arithmetic: 12.7 us -> 0 us
  local copies, waits for them, and re-layouts: 9.02 us -> 2.57 us
  matrix products: 3.48 us -> 0 us
    psum x2 -> x0, blocking collectives: 79.9 us -> none  [one_axis_at_a_time(): return functools.reduce(lax.psum, axes, x)]
    all_gather x1 -> x0, waiting for transfers between devices: 74.5 us -> none  [gathered_once(): both, at, found = (lax.all_gather(jnp.concatenate(lines), axis), 0, {})]
    pallas_call x0 -> x1, Pallas kernels: none -> 58.6 us  [body(): pl.pallas_call(functools.partial(kernel, nz, ny), name='decode_step', out...]
    all_gather x2 -> x0, blocking collectives: 38.7 us -> none  [the longest x1 20.4 us: gathered_once(): both, at, found = (lax.all_gather(jnp.concatenate(lines), axis), 0, {})]
    squeeze x48 -> x0, local copies, waits for them, and re-layouts: 6.09 us -> none  [the longest x42 5.33 us: joined_all(): x = combine(x, jax.tree.map(lambda part: part[k], pieces))]
    exp x12 -> x0, other arithmetic: 5.69 us -> none  [the longest x7 4.93 us: combine_parts(): factor_second = jnp.exp(highest_second - highest)]
    dot_general x7 -> x0, matrix products: 3.48 us -> none  [the longest x1 0.89 us: body(): jnp.dot(tokens, query_weight, preferred_element_type=jnp.float32)]
    add x3 -> x0, other arithmetic: 2.8 us -> none  [the longest x1 1.86 us: combine_parts(): weighted_first * factor_first[..., None]]
  transfers between devices with their start and end apart: 1 -> 0, of which waited for: 1 -> 0; matrix products, arithmetic and copies ran while one was open for 1% -> 0% of each run, Pallas kernels for 0% -> 0%
where the time goes in v1:
time: 62.1 us; the launch traced here: 61.9 us
  Pallas kernels  58.6 us (94%)
  local copies, waits for them, and re-layouts  2.57 us (4%)
  between operations  0.65 us (1%)
    pallas_call x1, Pallas kernels, body(): pl.pallas_call(functools.partial(kernel, nz, ny), name='decode_step', out...  58.6 us
    unnamed x9, local copies, waits for them, and re-layouts  2.57 us

profile of v1, /device:TPU:1, one launch (start us, length us, event | category | flops | bytes accessed | tf_op | source)
XLA Modules:
  0.0 61.9 jit_solution(9408092250143389400)
XLA Ops:
  0.6 58.6 %decode_step.1 = (bf16[8,16]{1,0:T(8,128)(2,1)}, bf16[8,128]{1,0:T(8,128)(2,1)}, bf16[8,128]{1,0:T(8,128)(2,1)}) custom-call(bf16[8,16]{1,0:T(8,128)(2,1)} %tok_hbm.1, s32[8]{0:T(128)} %len_hbm.1, bf16[16,1024]{1,0:T(8,128)(2,1)} %wq_hbm.1, bf16[16,128]{1,0:T(8,128)(2,1)} %wk_hbm.1, bf16[16,128]{1,0:T(8,128)(2,1)} %wv_hbm.1, f32[1,64]{1,0:T(1,128)} %bitcast.13, ...), custom_call_target="tpu_custom_call" | custom-call | tf_op jit(solution)/shard_map/decode_step/pallas_call | solution.py:366
  59.3 0.0 copy-start.2
  59.3 0.6 %copy-done.2 = bf16[8,16]{1,0:T(8,128)(2,1)S(1)} copy-done((bf16[8,16]{1,0:T(8,128)(2,1)S(1)}, bf16[8,16]{1,0:T(8,128)(2,1)}, u32[]{:S(2)}) %copy-start.2) | copy-done | bytes 280
  59.9 0.0 copy-start.1
  59.9 0.6 copy.19
  60.5 0.1 copy-done.1
  60.6 0.0 copy-start
  60.6 0.6 copy.20
  61.2 0.1 copy-done
  61.3 0.6 copy.21
Async XLA Ops:
  59.3 0.7 %copy-start.2 = (bf16[8,16]{1,0:T(8,128)(2,1)S(1)}, bf16[8,16]{1,0:T(8,128)(2,1)}, u32[]{:S(2)}) copy-start(bf16[8,16]{1,0:T(8,128)(2,1)} %get-tuple-element.12) | copy-start | bytes 772
  59.9 0.7 %copy-start.1 = (bf16[8,128]{1,0:T(8,128)(2,1)S(1)}, bf16[8,128]{1,0:T(8,128)(2,1)}, u32[]{:S(2)}) copy-start(bf16[8,128]{1,0:T(8,128)(2,1)} %get-tuple-element.7) | copy-start | bytes 6148
  60.6 0.7 %copy-start = (bf16[8,128]{1,0:T(8,128)(2,1)S(1)}, bf16[8,128]{1,0:T(8,128)(2,1)}, u32[]{:S(2)}) copy-start(bf16[8,128]{1,0:T(8,128)(2,1)} %get-tuple-element.8) | copy-start | bytes 6148

commit v2 on v1

--- a/solution.py
+++ b/solution.py
@@ -45,9 +45,7 @@
     ck_hbm,
     cv_hbm,
     freq_hbm,
-    mixed_ref,
-    nk_ref,
-    nv_ref,
+    out_ref,
     tok,
     wts,
     lens,
@@ -68,12 +66,11 @@
     zw,
     zst,
     attbuf,
-    tsend,
-    trecv,
     load_sem,
     send_sem,
     recv_sem,
     q_sem,
+    reach_sem,
 ):
     y = lax.axis_index("kv_1")
     z = lax.axis_index("kv_0")
@@ -87,10 +84,13 @@
         return lax.rem(z + k, nz)
 
     barrier = pltpu.get_barrier_semaphore()
-    for k in far_first(nz):
-        pl.semaphore_signal(barrier, 1, device_id={"kv_0": z_at(k)}, device_id_type=MESH)
     for k in far_first(ny):
         pl.semaphore_signal(barrier, 1, device_id={"kv_1": y_at(k)}, device_id_type=MESH)
+        pl.semaphore_signal(
+            barrier, 1, device_id={"kv_1": y_at(k), "tp": 1 - core}, device_id_type=MESH
+        )
+    for k in (1, nz - 1):
+        pl.semaphore_signal(barrier, 1, device_id={"kv_0": z_at(k)}, device_id_type=MESH)
     pl.semaphore_signal(barrier, 1, device_id={"tp": 1 - core}, device_id_type=MESH)
 
     width_q = wq_hbm.shape[1]
@@ -114,20 +114,31 @@
         loads.append(
             pltpu.make_async_copy(
                 ow_hbm.at[:, pl.ds(128 * h, 128)],
-                outw.at[pl.ds(columns * h, columns)],
+                outw.at[core, pl.ds(columns * h, columns)],
                 load_sem.at[12 + h],
             )
         )
     for load in loads:
         load.start()
 
-    def send(src, dst, which, axis, target, recv=None):
+    def tell(round_number, reach):
+        if round_number > 0:
+            pl.semaphore_wait(reach_sem.at[round_number - 1], 2)
+        for k in (reach, nz - reach):
+            pl.semaphore_signal(
+                reach_sem.at[round_number],
+                1,
+                device_id={"kv_0": z_at(k)},
+                device_id_type=MESH,
+            )
+
+    def send(src, dst, which, target, recv=None):
         copy = pltpu.make_async_remote_copy(
             src_ref=src,
             dst_ref=dst,
             send_sem=send_sem.at[which],
             recv_sem=recv_sem.at[which] if recv is None else recv,
-            device_id={axis: target},
+            device_id=target,
             device_id_type=MESH,
         )
         copy.start()
@@ -149,10 +160,12 @@
     for c in range(blocks):
         pbuf[:, c, :] = partial[:, 128 * c : 128 * (c + 1)]
 
-    pl.semaphore_wait(barrier, (ny - 1) + (nz - 1) + 1)
+    pl.semaphore_wait(barrier, 2 * (ny - 1) + 2 + 1)
 
     for k in far_first(ny):
-        send(pbuf.at[y_at(k)], yrecv.at[k - 1], 0, "kv_1", y_at(k))
+        send(pbuf.at[y_at(k)], yrecv.at[k - 1], 0, {"kv_1": y_at(k)})
+    if nz > 2:
+        tell(0, 1)
 
     for load in loads[4:10]:
         load.wait()
@@ -169,6 +182,17 @@
     for h in range(heads):
         lam = jnp.where(head_row == h, lams[h], lam)
 
+    reach, round_number = 2, 1
+    while reach < nz // 2:
+        tell(round_number, reach)
+        reach, round_number = 2 * reach, round_number + 1
+    if nz > 2:
+        pl.semaphore_wait(reach_sem.at[round_number - 1], 2)
+
+    for load in loads[12:]:
+        load.wait()
+    send(outw.at[core], outw.at[core], 8, {"tp": 1 - core})
+
     all_of(yrecv, 0).wait_recv()
     total = pbuf[y]
     for k in range(ny - 1):
@@ -176,7 +200,7 @@
 
     zbuf[z] = total
     for k in far_first(nz):
-        send(zbuf.at[z], zbuf.at[z], 1, "kv_0", z_at(k))
+        send(zbuf.at[z], zbuf.at[z], 1, {"kv_0": z_at(k)})
     all_of(zbuf.at[pl.ds(0, nz - 1)], 1).wait_recv()
     proj = zbuf[0]
     for k in range(1, nz):
@@ -195,9 +219,9 @@
     qbuf[y] = rotated[:heads].astype(BF16)
     kvbuf[y] = jnp.concatenate([rotated[heads : heads + 1], proj[heads + 1 :]], axis=0)
     for k in far_first(ny):
-        send(qbuf.at[y], qbuf.at[y], 2, "kv_1", y_at(k), q_sem.at[k - 1])
+        send(qbuf.at[y], qbuf.at[y], 2, {"kv_1": y_at(k)}, q_sem.at[k - 1])
     for k in far_first(ny):
-        send(kvbuf.at[y], kvbuf.at[y], 3, "kv_1", y_at(k))
+        send(kvbuf.at[y], kvbuf.at[y], 3, {"kv_1": y_at(k)})
 
     scale = 64 ** (-0.5)
     rows2 = 2 * heads
@@ -249,7 +273,7 @@
             device_id_type=MESH,
         ).wait_recv()
         attend(s)
-        send(bmsg.at[s], brecv.at[k - 1], 4, "kv_1", s)
+        send(bmsg.at[s], brecv.at[k - 1], 4, {"kv_1": s})
 
     own_query = two_maps(qbuf[y].astype(F32))
     own_key = kvbuf[y, pl.ds(0, 1), :].astype(BF16).astype(F32)
@@ -269,8 +293,8 @@
     zw[z] = weighted.astype(BF16)
     zst[z] = jnp.concatenate([high, count], axis=0)
     for k in far_first(nz):
-        send(zst.at[z], zst.at[z], 6, "kv_0", z_at(k))
-        send(zw.at[z], zw.at[z], 5, "kv_0", z_at(k))
+        send(zst.at[z], zst.at[z], 6, {"kv_0": z_at(k)})
+        send(zw.at[z], zw.at[z], 5, {"kv_0": z_at(k)})
     all_of(zst.at[pl.ds(0, nz - 1)], 6).wait_recv()
     stats = [zst[k] for k in range(nz)]
     high = own_score
@@ -292,35 +316,38 @@
     gaps = attention[:heads] - lam * attention[heads:]
     mean = jnp.sum(gaps * gaps, axis=1, keepdims=True) / 128
     attended = gaps * lax.rsqrt(mean + epsilon) * hgain[...] * output_scale
-    attbuf[y] = attended.astype(BF16)
+    attbuf[core * ny + y] = attended.astype(BF16)
+    mine = attbuf.at[core * ny + y]
     for k in far_first(ny):
-        send(attbuf.at[y], attbuf.at[y], 7, "kv_1", y_at(k))
+        send(mine, mine, 7, {"kv_1": y_at(k)})
+        send(mine, mine, 7, {"kv_1": y_at(k), "tp": 1 - core})
+    send(mine, mine, 7, {"tp": 1 - core})
 
     all_of(kvbuf.at[pl.ds(0, ny - 1)], 3).wait_recv()
     for s in range(ny):
-        nk_ref[pl.ds(s, 1), :] = kvbuf[s, pl.ds(0, 1), :].astype(BF16)
-        nv_ref[pl.ds(s, 1), :] = kvbuf[s, pl.ds(1, 1), :].astype(BF16)
-    for load in loads[12:]:
-        load.wait()
-
-    all_of(attbuf.at[pl.ds(0, ny - 1)], 7).wait_recv()
-    rows = jnp.concatenate([attbuf[s].astype(F32) for s in range(ny)], axis=0).astype(BF16)
-    product = lax.dot_general(
-        rows, outw[...], (((1,), (1,)), ((), ())), preferred_element_type=F32
-    )
-    out_row = lax.broadcasted_iota(jnp.int32, product.shape, 0)
-    out_lane = lax.broadcasted_iota(jnp.int32, product.shape, 1)
-    product = jnp.where(lax.rem(out_row, heads) == out_lane // columns, product, 0.0)
-    summed = jnp.sum(product.reshape(ny, heads, 128), axis=1)
-    step = columns
-    while step < 128:
-        summed = summed + pltpu.roll(summed, step, 1)
-        step *= 2
-    tsend[...] = summed.astype(BF16)
-    send(tsend, trecv, 8, "tp", 1 - core)
-    all_of(trecv, 8).wait_recv()
-    mixed = tsend[...].astype(F32) + trecv[...].astype(F32)
-    mixed_ref[...] = mixed[:, :columns].astype(BF16)
+        out_ref[pl.ds(s, 1), pl.ds(128, 128)] = kvbuf[s, pl.ds(0, 1), :]
+        out_ref[pl.ds(s, 1), pl.ds(256, 128)] = kvbuf[s, pl.ds(1, 1), :]
+    all_of(outw.at[0], 8).wait_recv()
+
+    all_of(attbuf.at[pl.ds(0, 2 * ny - 1)], 7).wait_recv()
+    mixed = jnp.zeros((ny, 128), F32)
+    for group in range(2):
+        rows = jnp.concatenate(
+            [attbuf[group * ny + s].astype(F32) for s in range(ny)], axis=0
+        ).astype(BF16)
+        product = lax.dot_general(
+            rows, outw[group], (((1,), (1,)), ((), ())), preferred_element_type=F32
+        )
+        out_row = lax.broadcasted_iota(jnp.int32, product.shape, 0)
+        out_lane = lax.broadcasted_iota(jnp.int32, product.shape, 1)
+        product = jnp.where(lax.rem(out_row, heads) == out_lane // columns, product, 0.0)
+        summed = jnp.sum(product.reshape(ny, heads, 128), axis=1)
+        step = columns
+        while step < 128:
+            summed = summed + pltpu.roll(summed, step, 1)
+            step *= 2
+        mixed = mixed + summed.astype(BF16).astype(F32)
+    out_ref[:, pl.ds(0, 128)] = mixed
 
     for which, ref in (
         (0, yrecv),
@@ -330,10 +357,16 @@
         (4, brecv),
         (5, zw.at[pl.ds(0, nz - 1)]),
         (6, zst.at[pl.ds(0, nz - 1)]),
-        (7, attbuf.at[pl.ds(0, ny - 1)]),
-        (8, trecv),
+        (7, attbuf.at[pl.ds(0, 2 * ny - 1)]),
+        (8, outw.at[0]),
     ):
         all_of(ref, which).wait_send()
+
+
+def cut(x_ref, mixed_ref, nk_ref, nv_ref):
+    mixed_ref[...] = x_ref[:, : mixed_ref.shape[1]].astype(BF16)
+    nk_ref[...] = x_ref[:, 128:256].astype(BF16)
+    nv_ref[...] = x_ref[:, 256:].astype(BF16)
 
 
 def body(
@@ -363,16 +396,12 @@
     blocks = heads + 2
     any_space = pl.BlockSpec(memory_space=pl.ANY)
     vmem = pl.BlockSpec(memory_space=pltpu.VMEM)
-    mixed, new_keys, new_values = pl.pallas_call(
+    out = pl.pallas_call(
         functools.partial(kernel, nz, ny),
         name="decode_step",
-        out_shape=(
-            jax.ShapeDtypeStruct((sequences, columns), BF16),
-            jax.ShapeDtypeStruct((sequences, 128), BF16),
-            jax.ShapeDtypeStruct((sequences, 128), BF16),
-        ),
+        out_shape=pltpu.VMEM((sequences, 384), F32),
         in_specs=[any_space] * 13,
-        out_specs=(vmem, vmem, vmem),
+        out_specs=vmem,
         scratch_shapes=[
             pltpu.VMEM((sequences, depth), BF16),
             pltpu.VMEM((depth, width_q + 256), BF16),
@@ -381,7 +410,7 @@
             pltpu.SMEM((heads,), F32),
             pltpu.VMEM((1, 128), F32),
             pltpu.VMEM((1, 128), F32),
-            pltpu.VMEM((heads * columns, 128), BF16),
+            pltpu.VMEM((2, heads * columns, 128), BF16),
             pltpu.VMEM((sequences, positions, 128), BF16),
             pltpu.VMEM((sequences, positions, 128), BF16),
             pltpu.VMEM((sequences, blocks, 128), F32),
@@ -393,13 +422,12 @@
             pltpu.VMEM((ny - 1, rows2 + 2, 128), F32),
             pltpu.VMEM((nz, rows2, 128), BF16),
             pltpu.VMEM((nz, 2, 128), F32),
-            pltpu.VMEM((ny, heads, 128), BF16),
-            pltpu.VMEM((sequences, 128), BF16),
-            pltpu.VMEM((sequences, 128), BF16),
+            pltpu.VMEM((2 * ny, heads, 128), BF16),
             pltpu.SemaphoreType.DMA((12 + heads,)),
             pltpu.SemaphoreType.DMA((9,)),
             pltpu.SemaphoreType.DMA((9,)),
             pltpu.SemaphoreType.DMA((ny - 1,)),
+            pltpu.SemaphoreType.REGULAR((4,)),
         ],
         compiler_params=pltpu.CompilerParams(collective_id=0, has_side_effects=True),
     )(
@@ -417,6 +445,17 @@
         cache_values.reshape(sequences, positions, 128),
         freq,
     )
+    mixed, new_keys, new_values = pl.pallas_call(
+        cut,
+        name="cut",
+        out_shape=(
+            jax.ShapeDtypeStruct((sequences, columns), BF16),
+            jax.ShapeDtypeStruct((sequences, 128), BF16),
+            jax.ShapeDtypeStruct((sequences, 128), BF16),
+        ),
+        in_specs=[vmem],
+        out_specs=(vmem, vmem, vmem),
+    )(pltpu.with_memory_space_constraint(out, pltpu.VMEM))
     return (
         mixed,
         new_keys.reshape(sequences, 1, 128),

time: 62.1 us -> 59.2 us (0.953)
  local copies, waits for them, and re-layouts: 2.57 us -> 0 us
    unnamed x9 -> x0, local copies, waits for them, and re-layouts: 2.57 us -> none
    pallas_call x1, Pallas kernels: 58.6 us -> 57.8 us  [body(): pl.pallas_call(functools.partial(kernel, nz, ny), name='decode_step', out...]
where the time goes in v2:
time: 59.2 us; the launch traced here: 59 us
  Pallas kernels  58.4 us (99%)
  between operations  0.64 us (1%)
    pallas_call x1, Pallas kernels, body(): pl.pallas_call(functools.partial(kernel, nz, ny), name='decode_step', out...  57.8 us

profile of v2, /device:TPU:1, one launch (start us, length us, event | category | flops | bytes accessed | tf_op | source)
XLA Modules:
  0.0 59.0 jit_solution(15574709932436413057)
XLA Ops:
  0.6 57.8 %decode_step.1.x_ref = f32[8,384]{1,0:T(8,128)S(1)} custom-call(bf16[8,16]{1,0:T(8,128)(2,1)} %tok_hbm.1, s32[8]{0:T(128)} %len_hbm.1, bf16[16,1024]{1,0:T(8,128)(2,1)} %wq_hbm.1, bf16[16,128]{1,0:T(8,128)(2,1)} %wk_hbm.1, bf16[16,128]{1,0:T(8,128)(2,1)} %wv_hbm.1, f32[1,64]{1,0:T(1,128)} %bitcast.11, f32[1,64]{1,0:T(1,128)} %bitcast.12, f32[8]{0:T(128)} %lam_hbm.1, ...), custom_call_target="tpu_custom_call" | custom-call | tf_op jit(solution)/shard_map/decode_step/pallas_call | solution.py:399
  58.5 0.6 cut.1

commit v3 on v2

--- a/solution.py
+++ b/solution.py
@@ -25,8 +25,15 @@
     return sorted(range(1, n), key=lambda k: -min(k, n - k))
 
 
+STAY = 2
+
+
 def near_first(n):
-    return sorted(range(1, n), key=lambda k: min(k, n - k))
+    return [k for k in sorted(range(1, n), key=lambda k: min(k, n - k)) if min(k, n - k) <= STAY]
+
+
+def moved(n):
+    return [k for k in far_first(n) if min(k, n - k) > STAY]
 
 
 def kernel(
@@ -58,11 +65,16 @@
     cv,
     pbuf,
     yrecv,
+    zsend,
     zbuf,
     qbuf,
     kvbuf,
+    kfar,
+    vfar,
     bmsg,
     brecv,
+    zwsend,
+    zstsend,
     zw,
     zst,
     attbuf,
@@ -75,6 +87,7 @@
     y = lax.axis_index("kv_1")
     z = lax.axis_index("kv_0")
     core = lax.axis_index("tp")
+    other = 1 - core
     positions = ck.shape[1]
 
     def y_at(k):
@@ -87,11 +100,14 @@
     for k in far_first(ny):
         pl.semaphore_signal(barrier, 1, device_id={"kv_1": y_at(k)}, device_id_type=MESH)
         pl.semaphore_signal(
-            barrier, 1, device_id={"kv_1": y_at(k), "tp": 1 - core}, device_id_type=MESH
+            barrier, 1, device_id={"kv_1": y_at(k), "tp": other}, device_id_type=MESH
         )
     for k in (1, nz - 1):
         pl.semaphore_signal(barrier, 1, device_id={"kv_0": z_at(k)}, device_id_type=MESH)
-    pl.semaphore_signal(barrier, 1, device_id={"tp": 1 - core}, device_id_type=MESH)
+        pl.semaphore_signal(
+            barrier, 1, device_id={"kv_0": z_at(k), "tp": other}, device_id_type=MESH
+        )
+    pl.semaphore_signal(barrier, 1, device_id={"tp": other}, device_id_type=MESH)
 
     width_q = wq_hbm.shape[1]
     loads = [
@@ -149,7 +165,7 @@
             dst_ref=ref,
             send_sem=send_sem.at[which],
             recv_sem=recv_sem.at[which],
-            device_id={"tp": 1 - core},
+            device_id={"tp": other},
             device_id_type=MESH,
         )
 
@@ -160,12 +176,17 @@
     for c in range(blocks):
         pbuf[:, c, :] = partial[:, 128 * c : 128 * (c + 1)]
 
-    pl.semaphore_wait(barrier, 2 * (ny - 1) + 2 + 1)
+    pl.semaphore_wait(barrier, 2 * (ny - 1) + 4 + 1)
 
     for k in far_first(ny):
-        send(pbuf.at[y_at(k)], yrecv.at[k - 1], 0, {"kv_1": y_at(k)})
+        send(pbuf.at[y_at(k)], yrecv.at[k], 0, {"kv_1": y_at(k), "tp": other})
+    send(pbuf.at[y], yrecv.at[0], 0, {"tp": other})
     if nz > 2:
         tell(0, 1)
+    for i, k in enumerate(moved(ny)):
+        send(ck_hbm.at[y_at(k)], kfar.at[i], 9, {"kv_1": y_at(k)})
+    for i, k in enumerate(moved(ny)):
+        send(cv_hbm.at[y_at(k)], vfar.at[i], 10, {"kv_1": y_at(k)})
 
     for load in loads[4:10]:
         load.wait()
@@ -191,17 +212,18 @@
 
     for load in loads[12:]:
         load.wait()
-    send(outw.at[core], outw.at[core], 8, {"tp": 1 - core})
+    send(outw.at[core], outw.at[core], 8, {"tp": other})
 
     all_of(yrecv, 0).wait_recv()
-    total = pbuf[y]
-    for k in range(ny - 1):
+    total = yrecv[0]
+    for k in range(1, ny):
         total = total + yrecv[k]
 
-    zbuf[z] = total
+    zsend[...] = total
     for k in far_first(nz):
-        send(zbuf.at[z], zbuf.at[z], 1, {"kv_0": z_at(k)})
-    all_of(zbuf.at[pl.ds(0, nz - 1)], 1).wait_recv()
+        send(zsend, zbuf.at[z], 1, {"kv_0": z_at(k), "tp": other})
+    send(zsend, zbuf.at[z], 1, {"tp": other})
+    all_of(zbuf, 1).wait_recv()
     proj = zbuf[0]
     for k in range(1, nz):
         proj = proj + zbuf[k]
@@ -218,7 +240,8 @@
     rotated = normed * cosine + partner * sine
     qbuf[y] = rotated[:heads].astype(BF16)
     kvbuf[y] = jnp.concatenate([rotated[heads : heads + 1], proj[heads + 1 :]], axis=0)
-    for k in far_first(ny):
+    near = near_first(ny)
+    for k in reversed(near):
         send(qbuf.at[y], qbuf.at[y], 2, {"kv_1": y_at(k)}, q_sem.at[k - 1])
     for k in far_first(ny):
         send(kvbuf.at[y], kvbuf.at[y], 3, {"kv_1": y_at(k)})
@@ -229,9 +252,7 @@
     wide_row = lax.broadcasted_iota(jnp.int32, (rows2, 128), 0)
     eye = wide_lane == wide_row
     half_low = lax.broadcasted_iota(jnp.int32, (heads, 128), 1) < 64
-    position_ids = (z * ny + y) * positions + lax.broadcasted_iota(
-        jnp.int32, (rows2, positions), 1
-    )
+    position = lax.broadcasted_iota(jnp.int32, (rows2, positions), 1)
 
     def to_row(column):
         return jnp.sum(jnp.where(eye, column, 0.0), axis=0, keepdims=True)
@@ -244,25 +265,33 @@
             [jnp.where(half_low, query, 0.0), jnp.where(half_low, 0.0, query)], axis=0
         )
 
-    def attend(s):
+    def attend(s, blocks, out):
         query = two_maps(qbuf[s].astype(F32)).astype(BF16)
-        scores = (
-            lax.dot_general(query, ck[s], (((1,), (1,)), ((), ())), preferred_element_type=F32)
-            * scale
-        )
-        valid = position_ids < lens[s]
-        highest = jnp.max(jnp.where(valid, scores, masked_score), axis=1, keepdims=True)
-        expo = jnp.where(valid, jnp.exp(scores - highest), 0.0)
-        count = jnp.sum(expo, axis=1, keepdims=True)
-        bmsg[s, pl.ds(0, rows2), :] = jnp.dot(
-            expo.astype(BF16), cv[s], preferred_element_type=F32
-        )
-        bmsg[s, pl.ds(rows2, 2), :] = jnp.concatenate([to_row(highest), to_row(count)], axis=0)
+        scores, valid = [], []
+        for keys, _, where in blocks:
+            scores.append(
+                lax.dot_general(query, keys, (((1,), (1,)), ((), ())), preferred_element_type=F32)
+                * scale
+            )
+            valid.append(position < lens[s] - (z * ny + where) * positions)
+        highest = functools.reduce(
+            jnp.maximum, [jnp.where(v, x, masked_score) for v, x in zip(valid, scores)]
+        )
+        highest = jnp.max(highest, axis=1, keepdims=True)
+        expo = [jnp.where(v, jnp.exp(x - highest), 0.0) for v, x in zip(valid, scores)]
+        count = jnp.sum(functools.reduce(jnp.add, expo), axis=1, keepdims=True)
+        bmsg[out, pl.ds(0, rows2), :] = functools.reduce(
+            jnp.add,
+            [
+                jnp.dot(e.astype(BF16), values, preferred_element_type=F32)
+                for e, (_, values, _) in zip(expo, blocks)
+            ],
+        )
+        bmsg[out, pl.ds(rows2, 2), :] = jnp.concatenate([to_row(highest), to_row(count)], axis=0)
 
     for load in loads[10:12]:
         load.wait()
-    attend(y)
-    for k in near_first(ny):
+    for k in near:
         s = lax.rem(y + ny - k, ny)
         pltpu.make_async_remote_copy(
             src_ref=qbuf.at[s],
@@ -272,8 +301,19 @@
             device_id={"kv_1": s},
             device_id_type=MESH,
         ).wait_recv()
-        attend(s)
-        send(bmsg.at[s], brecv.at[k - 1], 4, {"kv_1": s})
+        attend(s, [(ck[s], cv[s], y)], s)
+        send(bmsg.at[s], brecv.at[near.index(k)], 4, {"kv_1": s, "tp": other})
+
+    all_of(kfar, 9).wait_recv()
+    all_of(vfar, 10).wait_recv()
+    attend(
+        y,
+        [(ck[y], cv[y], y)]
+        + [(kfar[i], vfar[i], lax.rem(y + ny - k, ny)) for i, k in enumerate(moved(ny))],
+        y,
+    )
+
+    send(bmsg.at[y], brecv.at[len(near)], 4, {"tp": other})
 
     own_query = two_maps(qbuf[y].astype(F32))
     own_key = kvbuf[y, pl.ds(0, 1), :].astype(BF16).astype(F32)
@@ -281,7 +321,7 @@
     own_score = to_row(jnp.sum(own_query * own_key, axis=1, keepdims=True) * scale)
 
     all_of(brecv, 4).wait_recv()
-    parts = [bmsg[y]] + [brecv[k] for k in range(ny - 1)]
+    parts = [brecv[i] for i in range(len(near) + 1)]
     highs = [part[rows2 : rows2 + 1] for part in parts]
     high = functools.reduce(jnp.maximum, highs)
     count = jnp.zeros_like(high)
@@ -290,12 +330,14 @@
         factor = jnp.exp(one - high)
         count = count + factor * part[rows2 + 1 :]
         weighted = weighted + to_column(factor) * part[:rows2]
-    zw[z] = weighted.astype(BF16)
-    zst[z] = jnp.concatenate([high, count], axis=0)
+    zwsend[...] = weighted.astype(BF16)
+    zstsend[...] = jnp.concatenate([high, count], axis=0)
     for k in far_first(nz):
-        send(zst.at[z], zst.at[z], 6, {"kv_0": z_at(k)})
-        send(zw.at[z], zw.at[z], 5, {"kv_0": z_at(k)})
-    all_of(zst.at[pl.ds(0, nz - 1)], 6).wait_recv()
+        send(zstsend, zst.at[z], 6, {"kv_0": z_at(k), "tp": other})
+        send(zwsend, zw.at[z], 5, {"kv_0": z_at(k), "tp": other})
+    send(zstsend, zst.at[z], 6, {"tp": other})
+    send(zwsend, zw.at[z], 5, {"tp": other})
+    all_of(zst, 6).wait_recv()
     stats = [zst[k] for k in range(nz)]
     high = own_score
     for stat in stats:
@@ -310,7 +352,7 @@
     share = 1.0 / count
     attention = to_column(own_weight * share) * own_value
     columns_of = [to_column(factor * share) for factor in factors]
-    all_of(zw.at[pl.ds(0, nz - 1)], 5).wait_recv()
+    all_of(zw, 5).wait_recv()
     for k in range(nz):
         attention = attention + columns_of[k] * zw[k].astype(F32)
     gaps = attention[:heads] - lam * attention[heads:]
@@ -320,8 +362,8 @@
     mine = attbuf.at[core * ny + y]
     for k in far_first(ny):
         send(mine, mine, 7, {"kv_1": y_at(k)})
-        send(mine, mine, 7, {"kv_1": y_at(k), "tp": 1 - core})
-    send(mine, mine, 7, {"tp": 1 - core})
+        send(mine, mine, 7, {"kv_1": y_at(k), "tp": other})
+    send(mine, mine, 7, {"tp": other})
 
     all_of(kvbuf.at[pl.ds(0, ny - 1)], 3).wait_recv()
     for s in range(ny):
@@ -351,14 +393,16 @@
 
     for which, ref in (
         (0, yrecv),
-        (1, zbuf.at[pl.ds(0, nz - 1)]),
-        (2, qbuf.at[pl.ds(0, ny - 1)]),
+        (1, zbuf),
+        (2, qbuf.at[pl.ds(0, len(near))]),
         (3, kvbuf.at[pl.ds(0, ny - 1)]),
         (4, brecv),
-        (5, zw.at[pl.ds(0, nz - 1)]),
-        (6, zst.at[pl.ds(0, nz - 1)]),
+        (5, zw),
+        (6, zst),
         (7, attbuf.at[pl.ds(0, 2 * ny - 1)]),
         (8, outw.at[0]),
+        (9, kfar),
+        (10, vfar),
     ):
         all_of(ref, which).wait_send()
 
@@ -414,18 +458,23 @@
             pltpu.VMEM((sequences, positions, 128), BF16),
             pltpu.VMEM((sequences, positions, 128), BF16),
             pltpu.VMEM((sequences, blocks, 128), F32),
-            pltpu.VMEM((ny - 1, blocks, 128), F32),
+            pltpu.VMEM((ny, blocks, 128), F32),
+            pltpu.VMEM((blocks, 128), F32),
             pltpu.VMEM((nz, blocks, 128), F32),
             pltpu.VMEM((ny, heads, 128), BF16),
             pltpu.VMEM((ny, 2, 128), F32),
+            pltpu.VMEM((len(moved(ny)), positions, 128), BF16),
+            pltpu.VMEM((len(moved(ny)), positions, 128), BF16),
             pltpu.VMEM((ny, rows2 + 2, 128), F32),
-            pltpu.VMEM((ny - 1, rows2 + 2, 128), F32),
+            pltpu.VMEM((len(near_first(ny)) + 1, rows2 + 2, 128), F32),
+            pltpu.VMEM((rows2, 128), BF16),
+            pltpu.VMEM((2, 128), F32),
             pltpu.VMEM((nz, rows2, 128), BF16),
             pltpu.VMEM((nz, 2, 128), F32),
             pltpu.VMEM((2 * ny, heads, 128), BF16),
             pltpu.SemaphoreType.DMA((12 + heads,)),
-            pltpu.SemaphoreType.DMA((9,)),
-            pltpu.SemaphoreType.DMA((9,)),
+            pltpu.SemaphoreType.DMA((11,)),
+            pltpu.SemaphoreType.DMA((11,)),
             pltpu.SemaphoreType.DMA((ny - 1,)),
             pltpu.SemaphoreType.REGULAR((4,)),
         ],

time: 59.2 us -> 56.8 us (0.959)
  Pallas kernels: 58.4 us -> 56 us
    pallas_call x1, Pallas kernels: 57.8 us -> 55.4 us  [body(): pl.pallas_call(functools.partial(kernel, nz, ny), name='decode_step', out...]
where the time goes in v3:
time: 56.8 us; the launch traced here: 56.7 us
  Pallas kernels  56 us (99%)
  between operations  0.64 us (1%)
    pallas_call x1, Pallas kernels, body(): pl.pallas_call(functools.partial(kernel, nz, ny), name='decode_step', out...  55.4 us

profile of v3, /device:TPU:1, one launch (start us, length us, event | category | flops | bytes accessed | tf_op | source)
XLA Modules:
  0.0 56.7 jit_solution(17358804615842109478)
XLA Ops:
  0.6 55.4 %decode_step.1.x_ref = f32[8,384]{1,0:T(8,128)S(1)} custom-call(bf16[8,16]{1,0:T(8,128)(2,1)} %tok_hbm.1, s32[8]{0:T(128)} %len_hbm.1, bf16[16,1024]{1,0:T(8,128)(2,1)} %wq_hbm.1, bf16[16,128]{1,0:T(8,128)(2,1)} %wk_hbm.1, bf16[16,128]{1,0:T(8,128)(2,1)} %wv_hbm.1, f32[1,64]{1,0:T(1,128)} %bitcast.11, f32[1,64]{1,0:T(1,128)} %bitcast.12, f32[8]{0:T(128)} %lam_hbm.1, ...), custom_call_target="tpu_custom_call" | custom-call | tf_op jit(solution)/shard_map/decode_step/pallas_call | solution.py:443
  56.1 0.6 %cut.1 = (bf16[8,16]{1,0:T(8,128)(2,1)}, bf16[8,128]{1,0:T(8,128)(2,1)}, bf16[8,128]{1,0:T(8,128)(2,1)}) custom-call(f32[8,384]{1,0:T(8,128)S(1)} %decode_step.1.x_ref), custom_call_target="tpu_custom_call" | custom-call | tf_op jit(solution)/shard_map/cut/pallas_call | solution.py:497

commit v4 on v3

--- a/solution.py
+++ b/solution.py
@@ -23,17 +23,6 @@
 
 def far_first(n):
     return sorted(range(1, n), key=lambda k: -min(k, n - k))
-
-
-STAY = 2
-
-
-def near_first(n):
-    return [k for k in sorted(range(1, n), key=lambda k: min(k, n - k)) if min(k, n - k) <= STAY]
-
-
-def moved(n):
-    return [k for k in far_first(n) if min(k, n - k) > STAY]
 
 
 def kernel(
@@ -69,8 +58,8 @@
     zbuf,
     qbuf,
     kvbuf,
-    kfar,
-    vfar,
+    kside,
+    vside,
     bmsg,
     brecv,
     zwsend,
@@ -82,7 +71,7 @@
     send_sem,
     recv_sem,
     q_sem,
-    reach_sem,
+    gate_sem,
 ):
     y = lax.axis_index("kv_1")
     z = lax.axis_index("kv_0")
@@ -98,16 +87,10 @@
 
     barrier = pltpu.get_barrier_semaphore()
     for k in far_first(ny):
-        pl.semaphore_signal(barrier, 1, device_id={"kv_1": y_at(k)}, device_id_type=MESH)
-        pl.semaphore_signal(
-            barrier, 1, device_id={"kv_1": y_at(k), "tp": other}, device_id_type=MESH
-        )
-    for k in (1, nz - 1):
-        pl.semaphore_signal(barrier, 1, device_id={"kv_0": z_at(k)}, device_id_type=MESH)
-        pl.semaphore_signal(
-            barrier, 1, device_id={"kv_0": z_at(k), "tp": other}, device_id_type=MESH
-        )
+        pl.semaphore_signal(barrier, 1, device_id={"kv_1": y_at(k), "tp": 1}, device_id_type=MESH)
     pl.semaphore_signal(barrier, 1, device_id={"tp": other}, device_id_type=MESH)
+    for k in far_first(nz):
+        pl.semaphore_signal(barrier, 1, device_id={"kv_0": z_at(k), "tp": 0}, device_id_type=MESH)
 
     width_q = wq_hbm.shape[1]
     loads = [
@@ -137,16 +120,8 @@
     for load in loads:
         load.start()
 
-    def tell(round_number, reach):
-        if round_number > 0:
-            pl.semaphore_wait(reach_sem.at[round_number - 1], 2)
-        for k in (reach, nz - reach):
-            pl.semaphore_signal(
-                reach_sem.at[round_number],
-                1,
-                device_id={"kv_0": z_at(k)},
-                device_id_type=MESH,
-            )
+    def tell_other(gate):
+        pl.semaphore_signal(gate_sem.at[gate], 1, device_id={"tp": other}, device_id_type=MESH)
 
     def send(src, dst, which, target, recv=None):
         copy = pltpu.make_async_remote_copy(
@@ -176,17 +151,27 @@
     for c in range(blocks):
         pbuf[:, c, :] = partial[:, 128 * c : 128 * (c + 1)]
 
-    pl.semaphore_wait(barrier, 2 * (ny - 1) + 4 + 1)
+    @pl.when(core == 1)
+    def _():
+        pl.semaphore_wait(barrier, 2 * (ny - 1) + 1)
+        tell_other(0)
+
+    @pl.when(core == 0)
+    def _():
+        pl.semaphore_wait(gate_sem.at[0], 1)
 
     for k in far_first(ny):
         send(pbuf.at[y_at(k)], yrecv.at[k], 0, {"kv_1": y_at(k), "tp": other})
     send(pbuf.at[y], yrecv.at[0], 0, {"tp": other})
-    if nz > 2:
-        tell(0, 1)
-    for i, k in enumerate(moved(ny)):
-        send(ck_hbm.at[y_at(k)], kfar.at[i], 9, {"kv_1": y_at(k)})
-    for i, k in enumerate(moved(ny)):
-        send(cv_hbm.at[y_at(k)], vfar.at[i], 10, {"kv_1": y_at(k)})
+    half = positions // 2
+    for d in (3, 2, 1):
+        for side, sign in ((0, 1), (1, ny - 1)):
+            target = {"kv_1": y_at(d * sign)}
+            s = y_at((d + 1) * sign)
+            rows_in = pl.ds(side * half, half) if d == 3 else pl.ds(0, positions)
+            rows_out = pl.ds((d - 1) * positions, half if d == 3 else positions)
+            send(ck_hbm.at[s, rows_in], kside.at[side, rows_out], 9 + side, target)
+            send(cv_hbm.at[s, rows_in], vside.at[side, rows_out], 11 + side, target)
 
     for load in loads[4:10]:
         load.wait()
@@ -203,12 +188,14 @@
     for h in range(heads):
         lam = jnp.where(head_row == h, lams[h], lam)
 
-    reach, round_number = 2, 1
-    while reach < nz // 2:
-        tell(round_number, reach)
-        reach, round_number = 2 * reach, round_number + 1
-    if nz > 2:
-        pl.semaphore_wait(reach_sem.at[round_number - 1], 2)
+    @pl.when(core == 0)
+    def _():
+        pl.semaphore_wait(barrier, 2 * (nz - 1) + 1)
+        tell_other(1)
+
+    @pl.when(core == 1)
+    def _():
+        pl.semaphore_wait(gate_sem.at[1], 1)
 
     for load in loads[12:]:
         load.wait()
@@ -240,8 +227,8 @@
     rotated = normed * cosine + partner * sine
     qbuf[y] = rotated[:heads].astype(BF16)
     kvbuf[y] = jnp.concatenate([rotated[heads : heads + 1], proj[heads + 1 :]], axis=0)
-    near = near_first(ny)
-    for k in reversed(near):
+    near = (1, ny - 1)
+    for k in near:
         send(qbuf.at[y], qbuf.at[y], 2, {"kv_1": y_at(k)}, q_sem.at[k - 1])
     for k in far_first(ny):
         send(kvbuf.at[y], kvbuf.at[y], 3, {"kv_1": y_at(k)})
@@ -254,6 +241,16 @@
     half_low = lax.broadcasted_iota(jnp.int32, (heads, 128), 1) < 64
     position = lax.broadcasted_iota(jnp.int32, (rows2, positions), 1)
 
+    def positions_of(where):
+        return position + (z * ny + where) * positions
+
+    def positions_beside(side):
+        parts = [positions_of(y)]
+        for d in (1, 2, 3):
+            parts.append(positions_of(y_at(d if side == 1 else ny - d)))
+        parts[3] = parts[3][:, side * half : (side + 1) * half]
+        return jnp.concatenate(parts, axis=1)
+
     def to_row(column):
         return jnp.sum(jnp.where(eye, column, 0.0), axis=0, keepdims=True)
 
@@ -265,33 +262,32 @@
             [jnp.where(half_low, query, 0.0), jnp.where(half_low, 0.0, query)], axis=0
         )
 
-    def attend(s, blocks, out):
+    def attend(s, blocks, where):
         query = two_maps(qbuf[s].astype(F32)).astype(BF16)
-        scores, valid = [], []
-        for keys, _, where in blocks:
-            scores.append(
-                lax.dot_general(query, keys, (((1,), (1,)), ((), ())), preferred_element_type=F32)
-                * scale
-            )
-            valid.append(position < lens[s] - (z * ny + where) * positions)
-        highest = functools.reduce(
-            jnp.maximum, [jnp.where(v, x, masked_score) for v, x in zip(valid, scores)]
-        )
-        highest = jnp.max(highest, axis=1, keepdims=True)
-        expo = [jnp.where(v, jnp.exp(x - highest), 0.0) for v, x in zip(valid, scores)]
-        count = jnp.sum(functools.reduce(jnp.add, expo), axis=1, keepdims=True)
-        bmsg[out, pl.ds(0, rows2), :] = functools.reduce(
-            jnp.add,
-            [
-                jnp.dot(e.astype(BF16), values, preferred_element_type=F32)
-                for e, (_, values, _) in zip(expo, blocks)
-            ],
-        )
-        bmsg[out, pl.ds(rows2, 2), :] = jnp.concatenate([to_row(highest), to_row(count)], axis=0)
+        scores = [
+            lax.dot_general(query, keys, (((1,), (1,)), ((), ())), preferred_element_type=F32)
+            for keys, _ in blocks
+        ]
+        scores = jnp.concatenate(scores, axis=1) * scale
+        valid = where < lens[s]
+        highest = jnp.max(jnp.where(valid, scores, masked_score), axis=1, keepdims=True)
+        expo = jnp.where(valid, jnp.exp(scores - highest), 0.0)
+        count = jnp.sum(expo, axis=1, keepdims=True)
+        expo = expo.astype(BF16)
+        at = 0
+        weighted = jnp.zeros((rows2, 128), F32)
+        for _, values in blocks:
+            part = expo[:, at : at + values.shape[0]]
+            weighted = weighted + jnp.dot(part, values, preferred_element_type=F32)
+            at += values.shape[0]
+        bmsg[s, pl.ds(0, rows2), :] = weighted
+        bmsg[s, pl.ds(rows2, 2), :] = jnp.concatenate([to_row(highest), to_row(count)], axis=0)
 
     for load in loads[10:12]:
         load.wait()
-    for k in near:
+    attend(y, [(ck[y], cv[y])], positions_of(y))
+    send(bmsg.at[y], brecv.at[2], 4, {"tp": other})
+    for side, k in ((1, 1), (0, ny - 1)):
         s = lax.rem(y + ny - k, ny)
         pltpu.make_async_remote_copy(
             src_ref=qbuf.at[s],
@@ -301,19 +297,11 @@
             device_id={"kv_1": s},
             device_id_type=MESH,
         ).wait_recv()
-        attend(s, [(ck[s], cv[s], y)], s)
-        send(bmsg.at[s], brecv.at[near.index(k)], 4, {"kv_1": s, "tp": other})
-
-    all_of(kfar, 9).wait_recv()
-    all_of(vfar, 10).wait_recv()
-    attend(
-        y,
-        [(ck[y], cv[y], y)]
-        + [(kfar[i], vfar[i], lax.rem(y + ny - k, ny)) for i, k in enumerate(moved(ny))],
-        y,
-    )
-
-    send(bmsg.at[y], brecv.at[len(near)], 4, {"tp": other})
+        all_of(kside.at[side], 9 + side).wait_recv()
+        all_of(vside.at[side], 11 + side).wait_recv()
+        blocks = [(ck[s], cv[s]), (kside[side], vside[side])]
+        attend(s, blocks, positions_beside(side))
+        send(bmsg.at[s], brecv.at[side], 4, {"kv_1": s, "tp": other})
 
     own_query = two_maps(qbuf[y].astype(F32))
     own_key = kvbuf[y, pl.ds(0, 1), :].astype(BF16).astype(F32)
@@ -401,8 +389,10 @@
         (6, zst),
         (7, attbuf.at[pl.ds(0, 2 * ny - 1)]),
         (8, outw.at[0]),
-        (9, kfar),
-        (10, vfar),
+        (9, kside.at[0]),
+        (10, kside.at[1]),
+        (11, vside.at[0]),
+        (12, vside.at[1]),
     ):
         all_of(ref, which).wait_send()
 
@@ -463,20 +453,20 @@
             pltpu.VMEM((nz, blocks, 128), F32),
             pltpu.VMEM((ny, heads, 128), BF16),
             pltpu.VMEM((ny, 2, 128), F32),
-            pltpu.VMEM((len(moved(ny)), positions, 128), BF16),
-            pltpu.VMEM((len(moved(ny)), positions, 128), BF16),
+            pltpu.VMEM((2, 5 * positions // 2, 128), BF16),
+            pltpu.VMEM((2, 5 * positions // 2, 128), BF16),
             pltpu.VMEM((ny, rows2 + 2, 128), F32),
-            pltpu.VMEM((len(near_first(ny)) + 1, rows2 + 2, 128), F32),
+            pltpu.VMEM((3, rows2 + 2, 128), F32),
             pltpu.VMEM((rows2, 128), BF16),
             pltpu.VMEM((2, 128), F32),
             pltpu.VMEM((nz, rows2, 128), BF16),
             pltpu.VMEM((nz, 2, 128), F32),
             pltpu.VMEM((2 * ny, heads, 128), BF16),
             pltpu.SemaphoreType.DMA((12 + heads,)),
-            pltpu.SemaphoreType.DMA((11,)),
-            pltpu.SemaphoreType.DMA((11,)),
+            pltpu.SemaphoreType.DMA((13,)),
+            pltpu.SemaphoreType.DMA((13,)),
             pltpu.SemaphoreType.DMA((ny - 1,)),
-            pltpu.SemaphoreType.REGULAR((4,)),
+            pltpu.SemaphoreType.REGULAR((2,)),
         ],
         compiler_params=pltpu.CompilerParams(collective_id=0, has_side_effects=True),
     )(

time: 56.8 us -> 54.4 us (0.958)
  Pallas kernels: 56 us -> 53.6 us
    pallas_call x1, Pallas kernels: 55.4 us -> 53 us  [body(): pl.pallas_call(functools.partial(kernel, nz, ny), name='decode_step', out...]
where the time goes in v4:
time: 54.4 us; the launch traced here: 54.3 us
  Pallas kernels  53.6 us (99%)
  between operations  0.64 us (1%)
    pallas_call x1, Pallas kernels, body(): pl.pallas_call(functools.partial(kernel, nz, ny), name='decode_step', out...  53 us

profile of v4, /device:TPU:1, one launch (start us, length us, event | category | flops | bytes accessed | tf_op | source)
XLA Modules:
  0.0 54.3 jit_solution(16836312323113207179)
XLA Ops:
  0.6 53.0 %decode_step.1.x_ref = f32[8,384]{1,0:T(8,128)S(1)} custom-call(bf16[8,16]{1,0:T(8,128)(2,1)} %tok_hbm.1, s32[8]{0:T(128)} %len_hbm.1, bf16[16,1024]{1,0:T(8,128)(2,1)} %wq_hbm.1, bf16[16,128]{1,0:T(8,128)(2,1)} %wk_hbm.1, bf16[16,128]{1,0:T(8,128)(2,1)} %wv_hbm.1, f32[1,64]{1,0:T(1,128)} %bitcast.11, f32[1,64]{1,0:T(1,128)} %bitcast.12, f32[8]{0:T(128)} %lam_hbm.1, ...), custom_call_target="tpu_custom_call" | custom-call | tf_op jit(solution)/shard_map/decode_step/pallas_call | solution.py:433
  53.7 0.6 %cut.1 = (bf16[8,16]{1,0:T(8,128)(2,1)}, bf16[8,128]{1,0:T(8,128)(2,1)}, bf16[8,128]{1,0:T(8,128)(2,1)}) custom-call(f32[8,384]{1,0:T(8,128)S(1)} %decode_step.1.x_ref), custom_call_target="tpu_custom_call" | custom-call | tf_op jit(solution)/shard_map/cut/pallas_call | solution.py:487

commit v5 on v4

--- a/solution.py
+++ b/solution.py
@@ -77,6 +77,7 @@
     z = lax.axis_index("kv_0")
     core = lax.axis_index("tp")
     other = 1 - core
+    late = nz * 5 // 8
     positions = ck.shape[1]
 
     def y_at(k):
@@ -164,14 +165,33 @@
         send(pbuf.at[y_at(k)], yrecv.at[k], 0, {"kv_1": y_at(k), "tp": other})
     send(pbuf.at[y], yrecv.at[0], 0, {"tp": other})
     half = positions // 2
-    for d in (3, 2, 1):
-        for side, sign in ((0, 1), (1, ny - 1)):
-            target = {"kv_1": y_at(d * sign)}
-            s = y_at((d + 1) * sign)
-            rows_in = pl.ds(side * half, half) if d == 3 else pl.ds(0, positions)
-            rows_out = pl.ds((d - 1) * positions, half if d == 3 else positions)
-            send(ck_hbm.at[s, rows_in], kside.at[side, rows_out], 9 + side, target)
-            send(cv_hbm.at[s, rows_in], vside.at[side, rows_out], 11 + side, target)
+    sides = ((0, 1), (1, ny - 1))
+    middle = ny // 2
+
+    def rows_at(reach):
+        return (middle - reach - 1) * positions + half
+
+    def move(reach):
+        for d in range(middle, reach, -1):
+            hops = d - reach
+            for side, sign in sides:
+                target = {"kv_1": y_at(hops * sign)}
+                s = y_at(d * sign)
+                rows_in = pl.ds(side * half, half) if d == middle else pl.ds(0, positions)
+                rows_out = pl.ds((hops - 1) * positions, half if d == middle else positions)
+                send(ck_hbm.at[s, rows_in], kside.at[side, rows_out], 9 + side, target)
+                send(cv_hbm.at[s, rows_in], vside.at[side, rows_out], 11 + side, target)
+
+    def by_row(step):
+        @pl.when(z < late)
+        def _():
+            step(1)
+
+        @pl.when(z >= late)
+        def _():
+            step(2)
+
+    by_row(move)
 
     for load in loads[4:10]:
         load.wait()
@@ -227,9 +247,14 @@
     rotated = normed * cosine + partner * sine
     qbuf[y] = rotated[:heads].astype(BF16)
     kvbuf[y] = jnp.concatenate([rotated[heads : heads + 1], proj[heads + 1 :]], axis=0)
-    near = (1, ny - 1)
-    for k in near:
-        send(qbuf.at[y], qbuf.at[y], 2, {"kv_1": y_at(k)}, q_sem.at[k - 1])
+
+    def ask(reach):
+        for e in range(reach, 0, -1):
+            for _, sign in sides:
+                k = e * sign % ny
+                send(qbuf.at[y], qbuf.at[y], 2, {"kv_1": y_at(k)}, q_sem.at[k - 1])
+
+    by_row(ask)
     for k in far_first(ny):
         send(kvbuf.at[y], kvbuf.at[y], 3, {"kv_1": y_at(k)})
 
@@ -244,11 +269,11 @@
     def positions_of(where):
         return position + (z * ny + where) * positions
 
-    def positions_beside(side):
+    def positions_beside(side, reach):
         parts = [positions_of(y)]
-        for d in (1, 2, 3):
-            parts.append(positions_of(y_at(d if side == 1 else ny - d)))
-        parts[3] = parts[3][:, side * half : (side + 1) * half]
+        for hops in range(1, middle - reach + 1):
+            parts.append(positions_of(y_at(hops if side == 1 else ny - hops)))
+        parts[-1] = parts[-1][:, side * half : (side + 1) * half]
         return jnp.concatenate(parts, axis=1)
 
     def to_row(column):
@@ -286,30 +311,47 @@
     for load in loads[10:12]:
         load.wait()
     attend(y, [(ck[y], cv[y])], positions_of(y))
-    send(bmsg.at[y], brecv.at[2], 4, {"tp": other})
-    for side, k in ((1, 1), (0, ny - 1)):
-        s = lax.rem(y + ny - k, ny)
-        pltpu.make_async_remote_copy(
-            src_ref=qbuf.at[s],
-            dst_ref=qbuf.at[s],
-            send_sem=send_sem.at[2],
-            recv_sem=q_sem.at[k - 1],
-            device_id={"kv_1": s},
-            device_id_type=MESH,
-        ).wait_recv()
-        all_of(kside.at[side], 9 + side).wait_recv()
-        all_of(vside.at[side], 11 + side).wait_recv()
-        blocks = [(ck[s], cv[s]), (kside[side], vside[side])]
-        attend(s, blocks, positions_beside(side))
-        send(bmsg.at[s], brecv.at[side], 4, {"kv_1": s, "tp": other})
+    send(bmsg.at[y], brecv.at[4], 4, {"tp": other})
+
+    def answer(reach):
+        for e in range(1, reach + 1):
+            for side, sign in sides:
+                k = e * sign % ny
+                s = y_at(k)
+                pltpu.make_async_remote_copy(
+                    src_ref=qbuf.at[s],
+                    dst_ref=qbuf.at[s],
+                    send_sem=send_sem.at[2],
+                    recv_sem=q_sem.at[ny - k - 1],
+                    device_id={"kv_1": s},
+                    device_id_type=MESH,
+                ).wait_recv()
+                blocks, where = [(ck[s], cv[s])], positions_of(y)
+                if e == reach:
+                    keys = kside.at[side, pl.ds(0, rows_at(reach))]
+                    values = vside.at[side, pl.ds(0, rows_at(reach))]
+                    all_of(keys, 9 + side).wait_recv()
+                    all_of(values, 11 + side).wait_recv()
+                    blocks.append((keys[...], values[...]))
+                    where = positions_beside(side, reach)
+                attend(s, blocks, where)
+                send(bmsg.at[s], brecv.at[2 * (e - 1) + side], 4, {"kv_1": s, "tp": other})
+        if reach == 1:
+            nothing = jnp.full((1, 128), masked_score, F32)
+            for slot in (2, 3):
+                brecv[slot, pl.ds(0, rows2), :] = jnp.zeros((rows2, 128), F32)
+                brecv[slot, pl.ds(rows2, 1), :] = nothing
+                brecv[slot, pl.ds(rows2 + 1, 1), :] = jnp.zeros((1, 128), F32)
+
+    by_row(answer)
 
     own_query = two_maps(qbuf[y].astype(F32))
     own_key = kvbuf[y, pl.ds(0, 1), :].astype(BF16).astype(F32)
     own_value = kvbuf[y, pl.ds(1, 1), :].astype(BF16).astype(F32)
     own_score = to_row(jnp.sum(own_query * own_key, axis=1, keepdims=True) * scale)
 
-    all_of(brecv, 4).wait_recv()
-    parts = [brecv[i] for i in range(len(near) + 1)]
+    by_row(lambda reach: all_of(brecv.at[pl.ds(0, 2 * reach + 1)], 4).wait_recv())
+    parts = [brecv[i] for i in range(5)]
     highs = [part[rows2 : rows2 + 1] for part in parts]
     high = functools.reduce(jnp.maximum, highs)
     count = jnp.zeros_like(high)
@@ -320,11 +362,9 @@
         weighted = weighted + to_column(factor) * part[:rows2]
     zwsend[...] = weighted.astype(BF16)
     zstsend[...] = jnp.concatenate([high, count], axis=0)
-    for k in far_first(nz):
-        send(zstsend, zst.at[z], 6, {"kv_0": z_at(k), "tp": other})
-        send(zwsend, zw.at[z], 5, {"kv_0": z_at(k), "tp": other})
-    send(zstsend, zst.at[z], 6, {"tp": other})
-    send(zwsend, zw.at[z], 5, {"tp": other})
+    for target in range(nz):
+        send(zstsend, zst.at[z], 6, {"kv_0": target, "tp": other})
+        send(zwsend, zw.at[z], 5, {"kv_0": target, "tp": other})
     all_of(zst, 6).wait_recv()
     stats = [zst[k] for k in range(nz)]
     high = own_score
@@ -382,19 +422,22 @@
     for which, ref in (
         (0, yrecv),
         (1, zbuf),
-        (2, qbuf.at[pl.ds(0, len(near))]),
         (3, kvbuf.at[pl.ds(0, ny - 1)]),
-        (4, brecv),
         (5, zw),
         (6, zst),
         (7, attbuf.at[pl.ds(0, 2 * ny - 1)]),
         (8, outw.at[0]),
-        (9, kside.at[0]),
-        (10, kside.at[1]),
-        (11, vside.at[0]),
-        (12, vside.at[1]),
     ):
         all_of(ref, which).wait_send()
+
+    def drain(reach):
+        all_of(qbuf.at[pl.ds(0, 2 * reach)], 2).wait_send()
+        all_of(brecv.at[pl.ds(0, 2 * reach + 1)], 4).wait_send()
+        for side in range(2):
+            all_of(kside.at[side, pl.ds(0, rows_at(reach))], 9 + side).wait_send()
+            all_of(vside.at[side, pl.ds(0, rows_at(reach))], 11 + side).wait_send()
+
+    by_row(drain)
 
 
 def cut(x_ref, mixed_ref, nk_ref, nv_ref):
@@ -456,7 +499,7 @@
             pltpu.VMEM((2, 5 * positions // 2, 128), BF16),
             pltpu.VMEM((2, 5 * positions // 2, 128), BF16),
             pltpu.VMEM((ny, rows2 + 2, 128), F32),
-            pltpu.VMEM((3, rows2 + 2, 128), F32),
+            pltpu.VMEM((5, rows2 + 2, 128), F32),
             pltpu.VMEM((rows2, 128), BF16),
             pltpu.VMEM((2, 128), F32),
             pltpu.VMEM((nz, rows2, 128), BF16),

time: 54.4 us -> 53.3 us (0.980)
  Pallas kernels: 53.6 us -> 52.5 us
    pallas_call x1, Pallas kernels: 53 us -> 52 us  [body(): pl.pallas_call(functools.partial(kernel, nz, ny), name='decode_step', out...]
where the time goes in v5:
time: 53.3 us; the launch traced here: 53.2 us
  Pallas kernels  52.5 us (98%)
  between operations  0.64 us (1%)
    pallas_call x1, Pallas kernels, body(): pl.pallas_call(functools.partial(kernel, nz, ny), name='decode_step', out...  52 us

profile of v5, /device:TPU:1, one launch (start us, length us, event | category | flops | bytes accessed | tf_op | source)
XLA Modules:
  0.0 53.2 jit_solution(176604457541693027)
XLA Ops:
  0.6 52.0 %decode_step.1.x_ref = f32[8,384]{1,0:T(8,128)S(1)} custom-call(bf16[8,16]{1,0:T(8,128)(2,1)} %tok_hbm.1, s32[8]{0:T(128)} %len_hbm.1, bf16[16,1024]{1,0:T(8,128)(2,1)} %wq_hbm.1, bf16[16,128]{1,0:T(8,128)(2,1)} %wk_hbm.1, bf16[16,128]{1,0:T(8,128)(2,1)} %wv_hbm.1, f32[1,64]{1,0:T(1,128)} %bitcast.11, f32[1,64]{1,0:T(1,128)} %bitcast.12, f32[8]{0:T(128)} %lam_hbm.1, ...), custom_call_target="tpu_custom_call" | custom-call | tf_op jit(solution)/shard_map/decode_step/pallas_call | solution.py:476
  52.6 0.6 %cut.1 = (bf16[8,16]{1,0:T(8,128)(2,1)}, bf16[8,128]{1,0:T(8,128)(2,1)}, bf16[8,128]{1,0:T(8,128)(2,1)}) custom-call(f32[8,384]{1,0:T(8,128)S(1)} %decode_step.1.x_ref), custom_call_target="tpu_custom_call" | custom-call | tf_op jit(solution)/shard_map/cut/pallas_call | solution.py:530

commit v6 on v5

--- a/solution.py
+++ b/solution.py
@@ -56,6 +56,8 @@
     yrecv,
     zsend,
     zbuf,
+    qother,
+    kvother,
     qbuf,
     kvbuf,
     kside,
@@ -228,35 +230,66 @@
 
     zsend[...] = total
     for k in far_first(nz):
-        send(zsend, zbuf.at[z], 1, {"kv_0": z_at(k), "tp": other})
-    send(zsend, zbuf.at[z], 1, {"tp": other})
-    all_of(zbuf, 1).wait_recv()
-    proj = zbuf[0]
-    for k in range(1, nz):
-        proj = proj + zbuf[k]
-
-    low = lane < 64
-    squares = proj * proj
-    mean_low = jnp.sum(jnp.where(low, squares, 0.0), axis=1, keepdims=True) / 64
-    mean_high = jnp.sum(jnp.where(low, 0.0, squares), axis=1, keepdims=True) / 64
-    inverse = jnp.where(low, lax.rsqrt(mean_low + epsilon), lax.rsqrt(mean_high + epsilon))
-    normed = proj * inverse * gain
-    partner = jnp.where(
-        lax.rem(lane, 64) < 32, -pltpu.roll(normed, 96, 1), pltpu.roll(normed, 32, 1)
-    )
-    rotated = normed * cosine + partner * sine
-    qbuf[y] = rotated[:heads].astype(BF16)
-    kvbuf[y] = jnp.concatenate([rotated[heads : heads + 1], proj[heads + 1 :]], axis=0)
+        send(zsend, zbuf.at[other * nz + z], 1, {"kv_0": z_at(k), "tp": 1})
+
+    @pl.when(core == 0)
+    def _():
+        send(zsend, zbuf.at[other * nz + z], 1, {"tp": 1})
+
+    @pl.when(core == 1)
+    def _():
+        zbuf[z] = total
+        all_of(zbuf.at[pl.ds(0, 2 * nz - 1)], 1).wait_recv()
+        low = lane < 64
+        for group in range(2):
+            proj = zbuf[group * nz]
+            for k in range(1, nz):
+                proj = proj + zbuf[group * nz + k]
+            squares = proj * proj
+            mean_low = jnp.sum(jnp.where(low, squares, 0.0), axis=1, keepdims=True) / 64
+            mean_high = jnp.sum(jnp.where(low, 0.0, squares), axis=1, keepdims=True) / 64
+            inverse = jnp.where(
+                low, lax.rsqrt(mean_low + epsilon), lax.rsqrt(mean_high + epsilon)
+            )
+            normed = proj * inverse * gain
+            partner = jnp.where(
+                lax.rem(lane, 64) < 32, -pltpu.roll(normed, 96, 1), pltpu.roll(normed, 32, 1)
+            )
+            rotated = normed * cosine + partner * sine
+            query = rotated[:heads].astype(BF16)
+            entry = jnp.concatenate(
+                [rotated[heads : heads + 1], proj[heads + 1 :]], axis=0
+            )
+            if group == 0:
+                qother[...] = query
+                kvother[...] = entry
+            else:
+                qbuf[y] = query
+                kvbuf[y] = entry
 
     def ask(reach):
-        for e in range(reach, 0, -1):
-            for _, sign in sides:
-                k = e * sign % ny
-                send(qbuf.at[y], qbuf.at[y], 2, {"kv_1": y_at(k)}, q_sem.at[k - 1])
+        @pl.when(core == 1)
+        def _():
+            for e in range(reach, 0, -1):
+                for _, sign in sides:
+                    k = e * sign % ny
+                    target = {"kv_1": y_at(k), "tp": 0}
+                    send(qother, qbuf.at[y], 14, target, q_sem.at[k - 1])
+            for e in range(reach, 0, -1):
+                for _, sign in sides:
+                    k = e * sign % ny
+                    send(qbuf.at[y], qbuf.at[y], 2, {"kv_1": y_at(k)}, q_sem.at[k - 1])
 
     by_row(ask)
-    for k in far_first(ny):
-        send(kvbuf.at[y], kvbuf.at[y], 3, {"kv_1": y_at(k)})
+
+    @pl.when(core == 1)
+    def _():
+        send(qother, qbuf.at[y], 15, {"tp": 0}, q_sem.at[ny - 1])
+        send(kvother, kvbuf.at[y], 13, {"tp": 0})
+        for k in far_first(ny):
+            target = {"kv_1": y_at(k), "tp": 0}
+            send(kvother, kvbuf.at[y], 16, target, recv_sem.at[3])
+            send(kvbuf.at[y], kvbuf.at[y], 3, {"kv_1": y_at(k)})
 
     scale = 64 ** (-0.5)
     rows2 = 2 * heads
@@ -310,6 +343,18 @@
 
     for load in loads[10:12]:
         load.wait()
+    @pl.when(core == 0)
+    def _():
+        pltpu.make_async_remote_copy(
+            src_ref=qother,
+            dst_ref=qbuf.at[y],
+            send_sem=send_sem.at[15],
+            recv_sem=q_sem.at[ny - 1],
+            device_id={"tp": other},
+            device_id_type=MESH,
+        ).wait_recv()
+        all_of(kvother, 13).wait_recv()
+
     attend(y, [(ck[y], cv[y])], positions_of(y))
     send(bmsg.at[y], brecv.at[4], 4, {"tp": other})
 
@@ -421,8 +466,6 @@
 
     for which, ref in (
         (0, yrecv),
-        (1, zbuf),
-        (3, kvbuf.at[pl.ds(0, ny - 1)]),
         (5, zw),
         (6, zst),
         (7, attbuf.at[pl.ds(0, 2 * ny - 1)]),
@@ -430,8 +473,24 @@
     ):
         all_of(ref, which).wait_send()
 
+    @pl.when(core == 0)
+    def _():
+        all_of(zbuf.at[pl.ds(0, nz)], 1).wait_send()
+
+    @pl.when(core == 1)
+    def _():
+        all_of(zbuf.at[pl.ds(0, nz - 1)], 1).wait_send()
+        all_of(qother, 15).wait_send()
+        all_of(kvother, 13).wait_send()
+        all_of(kvbuf.at[pl.ds(0, ny - 1)], 16).wait_send()
+        all_of(kvbuf.at[pl.ds(0, ny - 1)], 3).wait_send()
+
     def drain(reach):
-        all_of(qbuf.at[pl.ds(0, 2 * reach)], 2).wait_send()
+        @pl.when(core == 1)
+        def _():
+            all_of(qbuf.at[pl.ds(0, 2 * reach)], 2).wait_send()
+            all_of(qbuf.at[pl.ds(0, 2 * reach)], 14).wait_send()
+
         all_of(brecv.at[pl.ds(0, 2 * reach + 1)], 4).wait_send()
         for side in range(2):
             all_of(kside.at[side, pl.ds(0, rows_at(reach))], 9 + side).wait_send()
@@ -493,7 +552,9 @@
             pltpu.VMEM((sequences, blocks, 128), F32),
             pltpu.VMEM((ny, blocks, 128), F32),
             pltpu.VMEM((blocks, 128), F32),
-            pltpu.VMEM((nz, blocks, 128), F32),
+            pltpu.VMEM((2 * nz, blocks, 128), F32),
+            pltpu.VMEM((heads, 128), BF16),
+            pltpu.VMEM((2, 128), F32),
             pltpu.VMEM((ny, heads, 128), BF16),
             pltpu.VMEM((ny, 2, 128), F32),
             pltpu.VMEM((2, 5 * positions // 2, 128), BF16),
@@ -506,9 +567,9 @@
             pltpu.VMEM((nz, 2, 128), F32),
             pltpu.VMEM((2 * ny, heads, 128), BF16),
             pltpu.SemaphoreType.DMA((12 + heads,)),
-            pltpu.SemaphoreType.DMA((13,)),
-            pltpu.SemaphoreType.DMA((13,)),
-            pltpu.SemaphoreType.DMA((ny - 1,)),
+            pltpu.SemaphoreType.DMA((17,)),
+            pltpu.SemaphoreType.DMA((17,)),
+            pltpu.SemaphoreType.DMA((ny,)),
             pltpu.SemaphoreType.REGULAR((2,)),
         ],
         compiler_params=pltpu.CompilerParams(collective_id=0, has_side_effects=True),

time: 53.3 us -> 52.5 us (0.985)
  Pallas kernels: 52.5 us -> 51.7 us
    pallas_call x1, Pallas kernels: 52 us -> 51.1 us  [body(): pl.pallas_call(functools.partial(kernel, nz, ny), name='decode_step', out...]
where the time goes in v6:
time: 52.5 us; the launch traced here: 52.3 us
  Pallas kernels  51.7 us (98%)
  between operations  0.64 us (1%)
    pallas_call x1, Pallas kernels, body(): pl.pallas_call(functools.partial(kernel, nz, ny), name='decode_step', out...  51.1 us

profile of v6, /device:TPU:1, one launch (start us, length us, event | category | flops | bytes accessed | tf_op | source)
XLA Modules:
  0.0 52.3 jit_solution(12145311953526411766)
XLA Ops:
  0.6 51.1 %decode_step.1.x_ref = f32[8,384]{1,0:T(8,128)S(1)} custom-call(bf16[8,16]{1,0:T(8,128)(2,1)} %tok_hbm.1, s32[8]{0:T(128)} %len_hbm.1, bf16[16,1024]{1,0:T(8,128)(2,1)} %wq_hbm.1, bf16[16,128]{1,0:T(8,128)(2,1)} %wk_hbm.1, bf16[16,128]{1,0:T(8,128)(2,1)} %wv_hbm.1, f32[1,64]{1,0:T(1,128)} %bitcast.11, f32[1,64]{1,0:T(1,128)} %bitcast.12, f32[8]{0:T(128)} %lam_hbm.1, ...), custom_call_target="tpu_custom_call" | custom-call | tf_op jit(solution)/shard_map/decode_step/pallas_call | solution.py:535
  51.7 0.6 %cut.1 = (bf16[8,16]{1,0:T(8,128)(2,1)}, bf16[8,128]{1,0:T(8,128)(2,1)}, bf16[8,128]{1,0:T(8,128)(2,1)}) custom-call(f32[8,384]{1,0:T(8,128)S(1)} %decode_step.1.x_ref), custom_call_target="tpu_custom_call" | custom-call | tf_op jit(solution)/shard_map/cut/pallas_call | solution.py:591

commit v7 on v6

--- a/solution.py
+++ b/solution.py
@@ -117,7 +117,7 @@
             pltpu.make_async_copy(
                 ow_hbm.at[:, pl.ds(128 * h, 128)],
                 outw.at[core, pl.ds(columns * h, columns)],
-                load_sem.at[12 + h],
+                load_sem.at[12],
             )
         )
     for load in loads:
@@ -142,7 +142,7 @@
             src_ref=ref,
             dst_ref=ref,
             send_sem=send_sem.at[which],
-            recv_sem=recv_sem.at[which],
+            recv_sem=recv_sem.at[which % 14],
             device_id={"tp": other},
             device_id_type=MESH,
         )
@@ -219,8 +219,7 @@
     def _():
         pl.semaphore_wait(gate_sem.at[1], 1)
 
-    for load in loads[12:]:
-        load.wait()
+    pltpu.make_async_copy(outw.at[core], outw.at[core], load_sem.at[12]).wait()
     send(outw.at[core], outw.at[core], 8, {"tp": other})
 
     all_of(yrecv, 0).wait_recv()
@@ -444,6 +443,39 @@
         out_ref[pl.ds(s, 1), pl.ds(256, 128)] = kvbuf[s, pl.ds(1, 1), :]
     all_of(outw.at[0], 8).wait_recv()
 
+    for which, ref in (
+        (0, yrecv),
+        (5, zw),
+        (6, zst),
+        (8, outw.at[0]),
+    ):
+        all_of(ref, which).wait_send()
+
+    @pl.when(core == 0)
+    def _():
+        all_of(zbuf.at[pl.ds(0, nz)], 1).wait_send()
+
+    @pl.when(core == 1)
+    def _():
+        all_of(zbuf.at[pl.ds(0, nz - 1)], 1).wait_send()
+        all_of(qother, 15).wait_send()
+        all_of(kvother, 13).wait_send()
+        all_of(kvbuf.at[pl.ds(0, ny - 1)], 16).wait_send()
+        all_of(kvbuf.at[pl.ds(0, ny - 1)], 3).wait_send()
+
+    def drain(reach):
+        @pl.when(core == 1)
+        def _():
+            all_of(qbuf.at[pl.ds(0, 2 * reach)], 2).wait_send()
+            all_of(qbuf.at[pl.ds(0, 2 * reach)], 14).wait_send()
+
+        all_of(brecv.at[pl.ds(0, 2 * reach + 1)], 4).wait_send()
+        for side in range(2):
+            all_of(kside.at[side, pl.ds(0, rows_at(reach))], 9 + side).wait_send()
+            all_of(vside.at[side, pl.ds(0, rows_at(reach))], 11 + side).wait_send()
+
+    by_row(drain)
+
     all_of(attbuf.at[pl.ds(0, 2 * ny - 1)], 7).wait_recv()
     mixed = jnp.zeros((ny, 128), F32)
     for group in range(2):
@@ -464,39 +496,7 @@
         mixed = mixed + summed.astype(BF16).astype(F32)
     out_ref[:, pl.ds(0, 128)] = mixed
 
-    for which, ref in (
-        (0, yrecv),
-        (5, zw),
-        (6, zst),
-        (7, attbuf.at[pl.ds(0, 2 * ny - 1)]),
-        (8, outw.at[0]),
-    ):
-        all_of(ref, which).wait_send()
-
-    @pl.when(core == 0)
-    def _():
-        all_of(zbuf.at[pl.ds(0, nz)], 1).wait_send()
-
-    @pl.when(core == 1)
-    def _():
-        all_of(zbuf.at[pl.ds(0, nz - 1)], 1).wait_send()
-        all_of(qother, 15).wait_send()
-        all_of(kvother, 13).wait_send()
-        all_of(kvbuf.at[pl.ds(0, ny - 1)], 16).wait_send()
-        all_of(kvbuf.at[pl.ds(0, ny - 1)], 3).wait_send()
-
-    def drain(reach):
-        @pl.when(core == 1)
-        def _():
-            all_of(qbuf.at[pl.ds(0, 2 * reach)], 2).wait_send()
-            all_of(qbuf.at[pl.ds(0, 2 * reach)], 14).wait_send()
-
-        all_of(brecv.at[pl.ds(0, 2 * reach + 1)], 4).wait_send()
-        for side in range(2):
-            all_of(kside.at[side, pl.ds(0, rows_at(reach))], 9 + side).wait_send()
-            all_of(vside.at[side, pl.ds(0, rows_at(reach))], 11 + side).wait_send()
-
-    by_row(drain)
+    all_of(attbuf.at[pl.ds(0, 2 * ny - 1)], 7).wait_send()
 
 
 def cut(x_ref, mixed_ref, nk_ref, nv_ref):
@@ -566,9 +566,9 @@
             pltpu.VMEM((nz, rows2, 128), BF16),
             pltpu.VMEM((nz, 2, 128), F32),
             pltpu.VMEM((2 * ny, heads, 128), BF16),
-            pltpu.SemaphoreType.DMA((12 + heads,)),
+            pltpu.SemaphoreType.DMA((13,)),
             pltpu.SemaphoreType.DMA((17,)),
-            pltpu.SemaphoreType.DMA((17,)),
+            pltpu.SemaphoreType.DMA((14,)),
             pltpu.SemaphoreType.DMA((ny,)),
             pltpu.SemaphoreType.REGULAR((2,)),
         ],

time: 52.5 us -> 52.4 us (level)
  no operation moved by 1% of the time
where the time goes in v7:
time: 52.4 us; the launch traced here: 52.2 us
  Pallas kernels  51.6 us (98%)
  between operations  0.64 us (1%)
    pallas_call x1, Pallas kernels, body(): pl.pallas_call(functools.partial(kernel, nz, ny), name='decode_step', out...  51 us

profile of v7, /device:TPU:1, one launch (start us, length us, event | category | flops | bytes accessed | tf_op | source)
XLA Modules:
  0.0 52.2 jit_solution(13744137941925191875)
XLA Ops:
  0.6 51.0 %decode_step.1.x_ref = f32[8,384]{1,0:T(8,128)S(1)} custom-call(bf16[8,16]{1,0:T(8,128)(2,1)} %tok_hbm.1, s32[8]{0:T(128)} %len_hbm.1, bf16[16,1024]{1,0:T(8,128)(2,1)} %wq_hbm.1, bf16[16,128]{1,0:T(8,128)(2,1)} %wk_hbm.1, bf16[16,128]{1,0:T(8,128)(2,1)} %wv_hbm.1, f32[1,64]{1,0:T(1,128)} %bitcast.11, f32[1,64]{1,0:T(1,128)} %bitcast.12, f32[8]{0:T(128)} %lam_hbm.1, ...), custom_call_target="tpu_custom_call" | custom-call | tf_op jit(solution)/shard_map/decode_step/pallas_call | solution.py:535
  51.6 0.6 %cut.1 = (bf16[8,16]{1,0:T(8,128)(2,1)}, bf16[8,128]{1,0:T(8,128)(2,1)}, bf16[8,128]{1,0:T(8,128)(2,1)}) custom-call(f32[8,384]{1,0:T(8,128)S(1)} %decode_step.1.x_ref), custom_call_target="tpu_custom_call" | custom-call | tf_op jit(solution)/shard_map/cut/pallas_call | solution.py:591

commit v8 on v7

--- a/solution.py
+++ b/solution.py
@@ -92,8 +92,6 @@
     for k in far_first(ny):
         pl.semaphore_signal(barrier, 1, device_id={"kv_1": y_at(k), "tp": 1}, device_id_type=MESH)
     pl.semaphore_signal(barrier, 1, device_id={"tp": other}, device_id_type=MESH)
-    for k in far_first(nz):
-        pl.semaphore_signal(barrier, 1, device_id={"kv_0": z_at(k), "tp": 0}, device_id_type=MESH)
 
     width_q = wq_hbm.shape[1]
     loads = [
@@ -120,7 +118,11 @@
                 load_sem.at[12],
             )
         )
-    for load in loads:
+    for load in loads[:4]:
+        load.start()
+    for k in far_first(nz):
+        pl.semaphore_signal(barrier, 1, device_id={"kv_0": z_at(k), "tp": 0}, device_id_type=MESH)
+    for load in loads[4:]:
         load.start()
 
     def tell_other(gate):
@@ -410,6 +412,7 @@
         send(zstsend, zst.at[z], 6, {"kv_0": target, "tp": other})
         send(zwsend, zw.at[z], 5, {"kv_0": target, "tp": other})
     all_of(zst, 6).wait_recv()
+    all_of(zw, 5).wait_recv()
     stats = [zst[k] for k in range(nz)]
     high = own_score
     for stat in stats:
@@ -424,7 +427,6 @@
     share = 1.0 / count
     attention = to_column(own_weight * share) * own_value
     columns_of = [to_column(factor * share) for factor in factors]
-    all_of(zw, 5).wait_recv()
     for k in range(nz):
         attention = attention + columns_of[k] * zw[k].astype(F32)
     gaps = attention[:heads] - lam * attention[heads:]
@@ -433,9 +435,10 @@
     attbuf[core * ny + y] = attended.astype(BF16)
     mine = attbuf.at[core * ny + y]
     for k in far_first(ny):
-        send(mine, mine, 7, {"kv_1": y_at(k)})
-        send(mine, mine, 7, {"kv_1": y_at(k), "tp": other})
+        send(mine, mine, 7, {"kv_1": y_at(k), "tp": 1})
     send(mine, mine, 7, {"tp": other})
+    for k in far_first(ny):
+        send(mine, mine, 7, {"kv_1": y_at(k), "tp": 0})
 
     all_of(kvbuf.at[pl.ds(0, ny - 1)], 3).wait_recv()
     for s in range(ny):

time: 52.4 us -> 52.5 us (level)
  no operation moved by 1% of the time
where the time goes in v8:
time: 52.5 us; the launch traced here: 52.3 us
  Pallas kernels  51.7 us (98%)
  between operations  0.64 us (1%)
    pallas_call x1, Pallas kernels, body(): pl.pallas_call(functools.partial(kernel, nz, ny), name='decode_step', out...  51.1 us

profile of v8, /device:TPU:1, one launch (start us, length us, event | category | flops | bytes accessed | tf_op | source)
XLA Modules:
  0.0 52.3 jit_solution(9978672845049583060)
XLA Ops:
  0.6 51.1 %decode_step.1.x_ref = f32[8,384]{1,0:T(8,128)S(1)} custom-call(bf16[8,16]{1,0:T(8,128)(2,1)} %tok_hbm.1, s32[8]{0:T(128)} %len_hbm.1, bf16[16,1024]{1,0:T(8,128)(2,1)} %wq_hbm.1, bf16[16,128]{1,0:T(8,128)(2,1)} %wk_hbm.1, bf16[16,128]{1,0:T(8,128)(2,1)} %wv_hbm.1, f32[1,64]{1,0:T(1,128)} %bitcast.11, f32[1,64]{1,0:T(1,128)} %bitcast.12, f32[8]{0:T(128)} %lam_hbm.1, ...), custom_call_target="tpu_custom_call" | custom-call | tf_op jit(solution)/shard_map/decode_step/pallas_call | solution.py:538
  51.7 0.6 %cut.1 = (bf16[8,16]{1,0:T(8,128)(2,1)}, bf16[8,128]{1,0:T(8,128)(2,1)}, bf16[8,128]{1,0:T(8,128)(2,1)}) custom-call(f32[8,384]{1,0:T(8,128)S(1)} %decode_step.1.x_ref), custom_call_target="tpu_custom_call" | custom-call | tf_op jit(solution)/shard_map/cut/pallas_call | solution.py:594
